TPU v7x, 256 devices: a whole 4x4x8 slice. The times are simulated.
256 devices in a mesh: sp: 64 (over z, x, core), tp: 4 (over y).
Axes of the slice: x: 4, y: 4, z: 8, core: 2. Of those that a mesh axis runs over, the one named last changes fastest.
Arguments:
- moe_input: bfloat16 [8192, 2048], P('sp'), may hold values from -6 to 6
- out_cotangent: bfloat16 [8192, 2048], P('sp'), may hold values from -16 to 16
- routes: int32 [8192, 2], P('sp'), may hold values from 0 to 15, all different within a row; in each aligned block of 128 rows (0 to 127, 128 to 255, ...) at most 16 rows name the same one
- route_weight: float32 [8192, 2], P('sp'), may hold values from 0.2 to 1
- w_gate: bfloat16 [64, 2048, 896], P('sp', None, 'tp'), may hold values from -0.125 to 0.125
- w_up: bfloat16 [64, 2048, 896], P('sp', None, 'tp'), may hold values from -0.125 to 0.125
- w_down: bfloat16 [64, 896, 2048], P('sp', 'tp'), may hold values from -0.09375 to 0.09375
- out_proj: bfloat16 [2048, 1024], P(None, 'tp'), may hold values from -0.243067956 to 0.243067956
- conv_out: bfloat16 [8192, 1024], P('sp', 'tp'), may hold values from -17 to 17
- glu_value: bfloat16 [8192, 1024], P('sp', 'tp'), may hold values from -6 to 6
- glu_gate: bfloat16 [8192, 1024], P('sp', 'tp'), may hold values from -9 to 9
- taps: float32 [31, 1024], P(None, 'tp'), may hold values from -1 to 1
- norm_gain: float32 [1024], P('tp'), may hold values from 0.1 to 1.9
Outputs:
- grad_gate: bfloat16 [64, 2048, 896], P('sp', None, 'tp')
- grad_up: bfloat16 [64, 2048, 896], P('sp', None, 'tp')
- grad_down: bfloat16 [64, 896, 2048], P('sp', 'tp')
- grad_proj: float32 [2048, 1024], P('sp', 'tp')
- grad_glu_value: bfloat16 [8192, 1024], P('sp', 'tp')
- grad_glu_gate: bfloat16 [8192, 1024], P('sp', 'tp')
Inputs may be any that keep to these rules, and one draw needn't show every extreme that they name: `routes`: each token names two different experts. Within the 128 tokens of one index of sp no expert is named more than 16 times, a bound that some block reaches.
All inputs are finite; a program needn't handle non-finite values.
Results may differ from a plain program's by a relative error of at most 0.014.
Values may be sent and summed in bfloat16 or wider, within the bound.
A program may use at most 128 MiB of HBM per device.

v0:
```python
import jax
import jax.numpy as jnp
from jax import lax
from jax.sharding import PartitionSpec as P

DB = 1024
WIDTH = 31
SPAN = 4


def in_blocks(array, dim, size):
    lengths = array.shape
    blocks = array.reshape(*lengths[:dim], size, lengths[dim] // size, *lengths[dim + 1 :])
    return jnp.moveaxis(blocks, dim, 0)


def sum_at_owner(array, axis, dim):
    size = lax.axis_size(axis)
    blocks = lax.all_to_all(in_blocks(array, dim, size), axis, 0, 0, tiled=True)
    return jnp.sum(blocks.astype(jnp.float32), axis=0)


def side_by_side(arrays, axis, split_dim, concat_dim, along):
    both = jnp.concatenate(arrays, axis=along)
    whole, at, finished = (
        lax.all_to_all(both, axis, split_axis=split_dim, concat_axis=concat_dim, tiled=True),
        0,
        [],
    )
    for a in arrays:
        finished.append(lax.slice_in_dim(whole, at, at + a.shape[along], axis=along))
        at += a.shape[along]
    return tuple(finished)


def sent_to_all(array, axis):
    copies = jnp.broadcast_to(array, (lax.axis_size(axis), *array.shape))
    return lax.all_to_all(copies, axis, split_axis=0, concat_axis=0, tiled=True)


def laid_out(blocks, dim):
    blocks = jnp.moveaxis(blocks, 0, dim)
    lengths = blocks.shape
    return blocks.reshape(*lengths[:dim], lengths[dim] * lengths[dim + 1], *lengths[dim + 2 :])


def gather_directly(array, axis, dim):
    blocks = sent_to_all(array, axis)
    return laid_out(blocks, dim)


def from_behind(block, axis, distance):
    devices = range(lax.axis_size(axis))
    route = [(i - distance, i) for i in devices if i - distance in devices]
    return lax.ppermute(block, axis, route)


def swish_slope(pre, sig):
    return sig * (1.0 + pre * (1.0 - sig))


def route_places(routes, experts, capacity):
    flat_routes = routes.reshape(-1)
    one_hot = (flat_routes[:, None] == jnp.arange(experts, dtype=jnp.int32)[None, :]).astype(
        jnp.int32
    )
    earlier = jnp.cumsum(one_hot, axis=0) - one_hot
    slot_index = jnp.sum(earlier * one_hot, axis=1)
    return flat_routes * capacity + slot_index


def expert_pass(expert_rows, expert_cot, w_gate, w_up, w_down):
    gate_w = w_gate[0]
    up_w = w_up[0]
    down_w = w_down[0]
    contract_rows = (((0,), (0,)), ((), ()))
    contract_units = (((1,), (1,)), ((), ()))
    gate_pre = jnp.dot(expert_rows, gate_w, preferred_element_type=jnp.float32)
    up_pre = jnp.dot(expert_rows, up_w, preferred_element_type=jnp.float32)
    gate_sig = jax.nn.sigmoid(gate_pre)
    hidden = (gate_pre * gate_sig * up_pre).astype(jnp.bfloat16)
    d_hidden = lax.dot_general(
        expert_cot, down_w, contract_units, preferred_element_type=jnp.float32
    )
    grad_down = lax.dot_general(
        hidden, expert_cot, contract_rows, preferred_element_type=jnp.float32
    ).astype(jnp.bfloat16)
    d_gate = (d_hidden * up_pre * swish_slope(gate_pre, gate_sig)).astype(jnp.bfloat16)
    d_up = (d_hidden * gate_pre * gate_sig).astype(jnp.bfloat16)
    grad_gate = lax.dot_general(
        expert_rows, d_gate, contract_rows, preferred_element_type=jnp.float32
    ).astype(jnp.bfloat16)
    grad_up = lax.dot_general(
        expert_rows, d_up, contract_rows, preferred_element_type=jnp.float32
    ).astype(jnp.bfloat16)
    total = lax.dot_general(gate_w, d_gate, contract_units, preferred_element_type=jnp.float32)
    summed = sum_at_owner(
        (
            total + lax.dot_general(up_w, d_up, contract_units, preferred_element_type=jnp.float32)
        ).astype(jnp.bfloat16),
        "tp",
        0,
    )
    return (grad_gate[None], grad_up[None], grad_down[None], summed.astype(jnp.bfloat16))


def local(
    moe_input,
    out_cotangent,
    routes,
    route_weight,
    w_gate,
    w_up,
    w_down,
    out_proj,
    conv_out,
    glu_value,
    glu_gate,
    taps,
    norm_gain,
):
    n_sp = lax.axis_size("sp")
    experts = n_sp // SPAN
    tok_rows = routes.shape[0]
    capacity = SPAN * min(tok_rows // SPAN, 2 * tok_rows // (experts * SPAN))
    model_width = moe_input.shape[1]
    target = route_places(routes, experts, capacity)
    matches = jnp.arange(experts * capacity, dtype=jnp.int32)[:, None] == target[None, :]
    token_ids = jnp.arange(2 * tok_rows, dtype=jnp.int32) // 2
    source = jnp.sum(jnp.where(matches, token_ids[None, :], 0), axis=1)
    weights = jnp.sum(jnp.where(matches, route_weight.reshape(-1)[None, :], 0.0), axis=1)
    filled = jnp.any(matches, axis=1)
    send_rows = jnp.where(filled[:, None], moe_input[source], jnp.zeros((), jnp.bfloat16))
    send_cot = (weights[:, None] * out_cotangent[source].astype(jnp.float32)).astype(jnp.bfloat16)
    copies_rows = jnp.broadcast_to(
        send_rows.reshape(experts, 1, capacity, model_width), (experts, SPAN, capacity, model_width)
    ).reshape(n_sp, capacity, model_width)
    copies_cot = jnp.broadcast_to(
        send_cot.reshape(experts, 1, capacity, model_width), (experts, SPAN, capacity, model_width)
    ).reshape(n_sp, capacity, model_width)
    recv_rows, recv_cot = side_by_side((copies_rows, copies_cot), "sp", 0, 0, 1)
    expert_rows = recv_rows.reshape(-1, model_width)
    expert_cot = recv_cot.reshape(-1, model_width)
    grad_gate, grad_up, grad_down, row_grads = expert_pass(
        expert_rows, expert_cot, w_gate, w_up, w_down
    )
    part_width = row_grads.shape[0]
    returned = lax.all_to_all(
        row_grads.reshape(part_width, n_sp, capacity), "sp", split_axis=1, concat_axis=1, tiled=True
    )
    slot_grads = jnp.sum(
        returned.astype(jnp.float32).reshape(part_width, experts, SPAN, capacity), axis=2
    ).reshape(part_width, experts * capacity)
    per_route = jnp.take(slot_grads, target, axis=1).reshape(part_width, tok_rows, 2)
    moe_grad = jnp.sum(per_route, axis=2)
    own_cot = lax.dynamic_slice_in_dim(
        out_cotangent, lax.axis_index("tp") * part_width, part_width, 1
    )
    resid_part = (own_cot.astype(jnp.float32).T + moe_grad).astype(jnp.bfloat16)
    resid_grad = gather_directly(resid_part, "tp", 0)
    conv_vals = conv_out.astype(jnp.float32)
    total_sum, square_sum = lax.psum(
        (jnp.sum(conv_vals, axis=1), jnp.sum(conv_vals * conv_vals, axis=1)), "tp"
    )
    mean = total_sum[:, None] / DB
    rstd = lax.rsqrt(square_sum[:, None] / DB - mean * mean + 1e-05)
    normed = (conv_vals - mean) * rstd
    zpre = normed * norm_gain[None, :]
    zsig = jax.nn.sigmoid(zpre)
    mixed = (zpre * zsig).astype(jnp.bfloat16)
    grad_proj = sum_at_owner(
        jnp.dot(resid_grad, mixed, preferred_element_type=jnp.float32).astype(jnp.bfloat16), "sp", 0
    )
    d_mixed = lax.dot_general(
        resid_grad, out_proj, (((0,), (0,)), ((), ())), preferred_element_type=jnp.float32
    )
    d_norm = d_mixed * swish_slope(zpre, zsig) * norm_gain[None, :]
    first_sum, second_sum = lax.psum(
        (jnp.sum(d_norm, axis=1), jnp.sum(d_norm * normed, axis=1)), "tp"
    )
    conv_grad = (
        rstd * (d_norm - first_sum[:, None] / DB - normed * second_sum[:, None] / DB)
    ).astype(jnp.bfloat16)
    later_rows = from_behind(conv_grad[: WIDTH - 1], "sp", -1)
    extended = jnp.concatenate([conv_grad, later_rows], axis=0).astype(jnp.float32)
    unit_grad = lax.conv_general_dilated(
        extended[None],
        taps[:, None, :],
        (1,),
        "VALID",
        dimension_numbers=("NWC", "WIO", "NWC"),
        feature_group_count=taps.shape[1],
        precision=lax.Precision.HIGHEST,
    )[0]
    gate_sig_in = jax.nn.sigmoid(glu_gate.astype(jnp.float32))
    grad_glu_value = (unit_grad * gate_sig_in).astype(jnp.bfloat16)
    grad_glu_gate = (
        unit_grad * glu_value.astype(jnp.float32) * gate_sig_in * (1.0 - gate_sig_in)
    ).astype(jnp.bfloat16)
    return (grad_gate, grad_up, grad_down, grad_proj, grad_glu_value, grad_glu_gate)


def solution(mesh):
    in_specs = (
        P("sp", None),
        P("sp", None),
        P("sp", None),
        P("sp", None),
        P("sp", None, "tp"),
        P("sp", None, "tp"),
        P("sp", "tp", None),
        P(None, "tp"),
        P("sp", "tp"),
        P("sp", "tp"),
        P("sp", "tp"),
        P(None, "tp"),
        P("tp"),
    )
    out_specs = (
        P("sp", None, "tp"),
        P("sp", None, "tp"),
        P("sp", "tp", None),
        P("sp", "tp"),
        P("sp", "tp"),
        P("sp", "tp"),
    )
    return jax.shard_map(local, mesh=mesh, in_specs=in_specs, out_specs=out_specs, check_vma=False)
```

profile of v0, /device:TPU:16, one launch (start us, length us, event | category | flops | bytes accessed | tf_op | source)
XLA Modules:
  0.0 375.7 jit_solution(5159150185069465004)
XLA Ops:
  0.6 0.0 copy-start
  0.6 0.9 copy.49
  1.5 0.1 reshape.186
  1.7 0.1 eq.40
  1.8 0.6 reduce-window.6
  2.4 0.2 slice_reduce_fusion
  2.6 0.1 fusion.50
  2.7 0.1 fusion.16
  2.9 0.1 select_reduce_fusion.2
  3.0 0.8 copy.52
  3.8 0.1 broadcast_in_dim.98
  3.9 0.1 select_reduce_fusion.1
  4.1 0.1 mul.144
  4.1 4.5 %gather_fusion.1 = bf16[256,2048]{1,0:T(8,128)(2,1)} fusion(bf16[128,2048]{1,0:T(8,128)(2,1)} %param.14, s32[1024]{0:T(1024)S(1)} %pad_clamp_fusion.1), kind=kCustom, calls=%fused_computation.1 | custom fusion | bytes 2098176 | tf_op jit(solution)/shard_map/gather | solution.py:134
  8.7 1.4 gather_fusion
  10.0 0.1 broadcast_in_dim.92
  10.1 1.5 fusion.3
  11.6 0.1 broadcast_select_fusion
  11.7 2.5 broadcast_in_dim.101
  14.2 2.5 broadcast_in_dim.97
  16.7 8.4 %pad_maximum_fusion = bf16[64,32,2048]{2,1,0:T(8,128)(2,1)} fusion(bf16[64,16,2048]{2,1,0:T(8,128)(2,1)} %bitcast.100, bf16[64,16,2048]{2,1,0:T(8,128)(2,1)} %bitcast.101), kind=kLoop, calls=%fused_computation.3 | loop fusion | flops 16777216 | bytes 16777216 | tf_op jit(solution)/shard_map/concatenate | solution.py:24
  25.1 198.1 %all_to_all.25 = bf16[64,32,2048]{2,1,0:T(8,128)(2,1)S(1)} all-to-all(bf16[64,32,2048]{2,1,0:T(8,128)(2,1)} %pad_maximum_fusion), channel_id=1, replica_groups=mesh['sp'=64,'tp'=4] {'sp'}, dimensions={0} | all-to-all | bytes 16777216 | tf_op jit(solution)/shard_map/all_to_all | solution.py:26
  223.2 1.2 fusion.55
  224.4 1.4 fusion.7
  225.8 0.5 copy-done.5
  226.3 1.4 fusion.10
  227.7 0.4 copy-done.12
  228.1 1.7 multiply_convert_fusion.1
  229.9 1.3 fusion.5
  231.2 1.3 add_convert_fusion
  232.6 0.4 copy.71
  233.0 49.4 %all_to_all.26 = bf16[4,512,1024]{1,2,0:T(8,128)(2,1)} all-to-all(bf16[4,512,1024]{1,2,0:T(8,128)(2,1)S(1)} %bitcast.99), channel_id=1, replica_groups=mesh['sp'=64,'tp'=4] {'tp'}, dimensions={0} | all-to-all | bytes 8388608 | tf_op jit(solution)/shard_map/all_to_all | solution.py:19
  282.3 4.2 %reduce_sum.113 = bf16[512,1024]{0,1:T(8,128)(2,1)} reduce(bf16[4,512,1024]{1,2,0:T(8,128)(2,1)} %all_to_all.26, bf16[]{:T(256)} %constant.59.clone.1), dimensions={0}, to_apply=%region_6.7 | reduce | flops 1572864 | bytes 5242882 | tf_op jit(solution)/shard_map/reduce_sum | solution.py:20
  286.5 6.6 %all-to-all-start.2 = ((bf16[512,64,16]{0,2,1:T(8,128)(2,1)}), bf16[512,64,16]{0,2,1:T(8,128)(2,1)S(1)}, u32[]{:S(2)}, u32[]{:S(2)}) async-start(bf16[512,64,16]{0,2,1:T(8,128)(2,1)} %bitcast.104), calls=%async_computation.2 | async-start | bytes 2097152 | tf_op jit(solution)/shard_map/all_to_all | solution.py:148
  293.2 0.1 reduce_sum.112
  293.3 0.1 copy.56
  293.5 0.1 mul.158
  293.6 0.1 copy.53
  293.7 0.1 copy.54
  293.8 0.1 convert_reduce_fusion.2
  294.0 8.9 %all-reduce.1 = (f32[128]{0:T(128)S(1)}, f32[128]{0:T(128)S(1)}) all-reduce(f32[128]{0:T(128)S(1)} %get-tuple-element.9, f32[128]{0:T(128)S(1)} %get-tuple-element.8), channel_id=1, replica_groups=mesh['sp'=64,'tp'=4] {'tp'}, use_global_device_ids=true, to_apply=%region_12.13 | all-reduce | flops 256 | bytes 2048 | tf_op jit(solution)/shard_map/psum | solution.py:162
  302.9 19.1 %all-to-all-done.2 = bf16[512,64,16]{0,2,1:T(8,128)(2,1)S(1)} async-done(((bf16[512,64,16]{0,2,1:T(8,128)(2,1)}), bf16[512,64,16]{0,2,1:T(8,128)(2,1)S(1)}, u32[]{:S(2)}, u32[]{:S(2)}) %all-to-all-start.2) | async-done | bytes 1048608 | tf_op jit(solution)/shard_map/all_to_all | solution.py:148
  322.0 0.2 convert_reduce_fusion
  322.2 1.0 gather_fusion.2
  323.2 0.3 gather.18
  323.5 0.7 select_reduce_fusion
  324.3 0.9 fusion.15
  325.2 0.1 copy.57
  325.3 0.9 broadcast_in_dim.107
  326.2 6.2 %all-to-all-start.3 = ((bf16[4,512,128]{2,1,0:T(8,128)(2,1)}), bf16[4,512,128]{2,1,0:T(8,128)(2,1)S(1)}, u32[]{:S(2)}, u32[]{:S(2)}) async-start(bf16[4,512,128]{2,1,0:T(8,128)(2,1)} %broadcast_in_dim.107), calls=%async_computation.3 | async-start | bytes 1048576 | tf_op jit(solution)/shard_map/all_to_all | solution.py:38
  332.4 4.8 %fusion = bf16[1,224,2048]{2,1,0:T(8,128)(2,1)} fusion(bf16[1024,2048]{1,0:T(8,128)(2,1)} %bitcast.110, f32[1024,224]{0,1:T(8,128)} %copy-done.15, f32[1024,224]{0,1:T(8,128)} %copy-done.14), kind=kOutput, calls=%fused_computation.10 | convolution fusion | flops 941359104 | bytes 6946816 | tf_op jit(solution)/shard_map/dot_general | solution.py:85
  337.2 1.6 all-to-all-done.3
  338.8 1.5 convolution_convert_fusion
  340.3 5.7 %all-to-all-start.4 = ((bf16[64,32,256]{2,1,0:T(8,128)(2,1)}), bf16[64,32,256]{2,1,0:T(8,128)(2,1)S(1)}, u32[]{:S(2)}, u32[]{:S(2)}) async-start(bf16[64,32,256]{2,1,0:T(8,128)(2,1)} %bitcast.24), calls=%async_computation.4 | async-start | bytes 2097152 | tf_op jit(solution)/shard_map/all_to_all | solution.py:19
  346.1 4.2 %fusion.1 = bf16[1,2048,224]{1,2,0:T(8,128)(2,1)} fusion(bf16[1024,224]{0,1:T(8,128)(2,1)S(1)} %get-tuple-element.17, bf16[1024,2048]{1,0:T(8,128)(2,1)} %bitcast.107), kind=kOutput, calls=%fused_computation.11 | convolution fusion | flops 939982848 | bytes 5570560 | tf_op jit(solution)/shard_map/dot_general | solution.py:90
  350.3 0.4 fusion.54
  350.7 9.2 %all-reduce = (f32[128]{0:T(128)S(1)}, f32[128]{0:T(128)S(1)}) all-reduce(f32[128]{0:T(128)S(1)} %get-tuple-element.7, f32[128]{0:T(128)S(1)} %get-tuple-element.6), channel_id=1, replica_groups=mesh['sp'=64,'tp'=4] {'tp'}, use_global_device_ids=true, to_apply=%region_17.18 | all-reduce | flops 256 | bytes 2048 | tf_op jit(solution)/shard_map/psum | solution.py:178
  359.9 0.1 fusion.36
  360.1 1.4 collective-permute-start
  361.5 4.4 %fusion.2 = bf16[1,2048,224]{1,2,0:T(8,128)(2,1)} fusion(bf16[1024,224]{0,1:T(8,128)(2,1)} %copy-done.7, bf16[1024,2048]{1,0:T(8,128)(2,1)} %bitcast.108), kind=kOutput, calls=%fused_computation.12 | convolution fusion | flops 939982848 | bytes 5570560 | tf_op jit(solution)/shard_map/dot_general | solution.py:93
  365.9 0.5 fusion.17
  366.5 0.7 fusion.41
  367.2 7.7 %all-to-all-done.4 = bf16[64,32,256]{2,1,0:T(8,128)(2,1)S(1)} async-done(((bf16[64,32,256]{2,1,0:T(8,128)(2,1)}), bf16[64,32,256]{2,1,0:T(8,128)(2,1)S(1)}, u32[]{:S(2)}, u32[]{:S(2)}) %all-to-all-start.4) | async-done | bytes 1048608 | tf_op jit(solution)/shard_map/all_to_all | solution.py:19
  374.9 0.8 convert_reduce_fusion.1
  (44 shorter events, 0.2 us)
Async XLA Ops:
  0.6 349.7 %copy-start = (bf16[2048,256]{1,0:T(8,128)(2,1)S(1)}, bf16[2048,256]{1,0:T(8,128)(2,1)}, u32[]{:S(2)}) copy-start(bf16[2048,256]{1,0:T(8,128)(2,1)} %param.20) | copy-start | bytes 3145732
  4.1 4.5 %copy-start.1 = (bf16[128,2048]{1,0:T(8,128)(2,1)S(1)}, bf16[128,2048]{1,0:T(8,128)(2,1)}, u32[]{:S(2)}) copy-start(bf16[128,2048]{1,0:T(8,128)(2,1)} %param.13) | copy-start | bytes 1572868
  223.2 1.2 copy-start.4
  224.4 3.3 copy-start.2
  224.4 3.3 copy-start.3
  224.4 1.9 copy-start.5
  226.3 3.6 copy-start.14
  226.3 1.8 copy-start.12
  227.7 2.2 copy-start.15
  229.9 1.3 copy-start.7
  282.3 11.0 %copy-start.10 = (s32[128,2]{0,1:T(2,128)S(1)}, s32[128,2]{0,1:T(2,128)}, u32[]{:S(2)}) copy-start(s32[128,2]{0,1:T(2,128)} %param.15) | copy-start | bytes 3076
  282.3 11.5 %copy-start.6 = (bf16[128,256]{1,0:T(8,128)(2,1)S(1)}, bf16[128,256]{1,0:T(8,128)(2,1)}, u32[]{:S(2)}) copy-start(bf16[128,256]{1,0:T(8,128)(2,1)} %param.21) | copy-start | bytes 196612
  286.5 35.5 %all-to-all-start.2 = ((bf16[512,64,16]{0,2,1:T(8,128)(2,1)}), bf16[512,64,16]{0,2,1:T(8,128)(2,1)S(1)}, u32[]{:S(2)}, u32[]{:S(2)}) async-start(bf16[512,64,16]{0,2,1:T(8,128)(2,1)} %bitcast.104), calls=%async_computation.2 | async-start | bytes 2097152 | tf_op jit(solution)/shard_map/all_to_all | solution.py:148
  326.2 12.6 %all-to-all-start.3 = ((bf16[4,512,128]{2,1,0:T(8,128)(2,1)}), bf16[4,512,128]{2,1,0:T(8,128)(2,1)S(1)}, u32[]{:S(2)}, u32[]{:S(2)}) async-start(bf16[4,512,128]{2,1,0:T(8,128)(2,1)} %broadcast_in_dim.107), calls=%async_computation.3 | async-start | bytes 1048576 | tf_op jit(solution)/shard_map/all_to_all | solution.py:38
  332.4 6.4 %copy-start.11 = (f32[256]{0:T(256)S(1)}, f32[256]{0:T(256)}, u32[]{:S(2)}) copy-start(f32[256]{0:T(256)} %param.25) | copy-start | bytes 3076
  340.3 34.6 %all-to-all-start.4 = ((bf16[64,32,256]{2,1,0:T(8,128)(2,1)}), bf16[64,32,256]{2,1,0:T(8,128)(2,1)S(1)}, u32[]{:S(2)}, u32[]{:S(2)}) async-start(bf16[64,32,256]{2,1,0:T(8,128)(2,1)} %bitcast.24), calls=%async_computation.4 | async-start | bytes 2097152 | tf_op jit(solution)/shard_map/all_to_all | solution.py:19
  350.3 15.6 %copy-start.13 = (f32[31,256]{1,0:T(8,128)S(1)}, f32[31,256]{1,0:T(8,128)}, u32[]{:S(2)}) copy-start(f32[31,256]{1,0:T(8,128)} %param.24) | copy-start | bytes 95236
  360.1 6.4 %copy-start.8 = (bf16[128,256]{1,0:T(8,128)(2,1)S(1)}, bf16[128,256]{1,0:T(8,128)(2,1)}, u32[]{:S(2)}) copy-start(bf16[128,256]{1,0:T(8,128)(2,1)} %param.22) | copy-start | bytes 196612
  360.1 6.4 %copy-start.9 = (bf16[128,256]{1,0:T(8,128)(2,1)S(1)}, bf16[128,256]{1,0:T(8,128)(2,1)}, u32[]{:S(2)}) copy-start(bf16[128,256]{1,0:T(8,128)(2,1)} %param.23) | copy-start | bytes 196612
  360.1 5.8 %collective-permute-start = (bf16[30,256]{1,0:T(8,128)(2,1)S(1)}, bf16[30,256]{1,0:T(8,128)(2,1)S(1)}, u32[]{:S(2)}, u32[]{:S(2)}) collective-permute-start(bf16[30,256]{1,0:T(8,128)(2,1)S(1)} %slice.29), channel_id=1, source_target_pairs={{4,0},{8,4},{12,8},{16,12},{20,16},{24,20},{28,24},{32,28},{36,32}... | collective-permute-start | bytes 46088 | tf_op jit(solution)/shard_map/ppermute | solution.py:55
where the time goes:
time: 380 us; the launch traced here: 376 us
  blocking collectives  266 us (70%)
  waiting for transfers between devices  28.4 us (7%)
  matrix products  23.1 us (6%)
  starting transfers between devices  19.9 us (5%)
  other arithmetic  18.9 us (5%)
  local copies, waits for them, and re-layouts  18.7 us (5%)
    all_to_all x1, blocking collectives, side_by_side(): lax.all_to_all(both, axis, split_axis=split_dim, concat_axis=concat_dim,...  198 us
    all_to_all x1, blocking collectives, sum_at_owner(): blocks = lax.all_to_all(in_blocks(array, dim, size), axis, 0, 0, tiled=True)  49.4 us
    all_to_all x1, waiting for transfers between devices, local(): lax.all_to_all(row_grads.reshape(part_width, n_sp, capacity), 'sp', split...  19.1 us
    psum x1, blocking collectives, local(): lax.psum((jnp.sum(d_norm, axis=1), jnp.sum(d_norm * normed, axis=1)), 'tp')  9.19 us
    psum x1, blocking collectives, local(): lax.psum((jnp.sum(conv_vals, axis=1), jnp.sum(conv_vals * conv_vals, axis...  8.94 us
    concatenate x1, other arithmetic, side_by_side(): both = jnp.concatenate(arrays, axis=along)  8.35 us
    all_to_all x1, waiting for transfers between devices, sum_at_owner(): blocks = lax.all_to_all(in_blocks(array, dim, size), axis, 0, 0, tiled=True)  7.73 us
  transfers between devices with their start and end apart: 4, of which 3 were waited for; matrix products, arithmetic and copies ran while one was open for 4% of the time, Pallas kernels for 0%

commit v1 on v0

v1 whole, which is shorter than its diff:
```python
import jax
import jax.numpy as jnp
from jax import lax
from jax.experimental import pallas as pl
from jax.experimental.pallas import tpu as pltpu
from jax.sharding import PartitionSpec as P

DB = 1024
WIDTH = 31
SPAN = 4
MESH = pl.DeviceIdType.MESH
BF = jnp.bfloat16
F32 = jnp.float32
NT = (((1,), (1,)), ((), ()))
NN = (((1,), (0,)), ((), ()))
TN = (((0,), (0,)), ((), ()))


def mm(a, b, dims):
    return lax.dot_general(a, b, dims, preferred_element_type=F32)


def swish_slope(pre, sig):
    return sig * (1.0 + pre * (1.0 - sig))


def expert_kernel(
    routes_ref, weight_ref, x_hbm, cot_hbm, wg_hbm, wu_hbm, wd_hbm,
    gg_hbm, gu_hbm, gd_hbm, res_ref,
    xq, cq, perm, sendbuf, xc, wg, wu, wd, act_t, dg_t, du_t, gout,
    part, sib_in, in_a, in_b, in_c, in_d, in_e, total, ret,
    load_sem, out_sem, own_sem, a2a_send, a2a_recv, ag_send, ag_recv,
    sb_send, sb_recv, rs_send, rs_recv, ret_send, ret_recv, res_send, res_recv,
):
    sp = lax.axis_index("sp")
    y = lax.axis_index("tp")
    c = lax.rem(sp, 2)
    x = lax.rem(sp // 2, 4)
    z = sp // 8
    xh = x // 2
    xl = lax.rem(x, 2)
    g = lax.rem(xl + xh, 2)
    og = 1 - g
    oc = 1 - c
    me = sp // 4
    yp, ym, y2 = lax.rem(y + 1, 4), lax.rem(y + 3, 4), lax.rem(y + 2, 4)

    def holder(q):
        qh = lax.rem(q, 2)
        qx = qh * 2 + lax.rem(g + qh, 2)
        return ((q // 2) * 8 + qx * 2 + c, y)

    dev_x = (z * 8 + (xh * 2 + 1 - xl) * 2 + c, y)
    dev_s = (z * 8 + x * 2 + oc, y)
    dev_p = (sp, yp)
    dev_m = (sp, ym)

    def remote(src, dst, ss, rs, dev):
        return pltpu.make_async_remote_copy(
            src_ref=src, dst_ref=dst, send_sem=ss, recv_sem=rs, device_id=dev,
            device_id_type=MESH,
        )

    barrier = pltpu.get_barrier_semaphore()

    def greet(k, _):
        pl.semaphore_signal(barrier, inc=1, device_id=holder(lax.rem(me + k, 16)), device_id_type=MESH)
        return 0

    lax.fori_loop(1, 16, greet, 0)
    for dev in (dev_x, dev_s, dev_p, dev_m):
        pl.semaphore_signal(barrier, inc=1, device_id=dev, device_id_type=MESH)

    cols = pl.ds(pl.multiple_of(y * 512, 512), 512)
    load_x = pltpu.make_async_copy(x_hbm.at[:, cols], xq, load_sem.at[0])
    load_c = pltpu.make_async_copy(cot_hbm.at[:, cols], cq, load_sem.at[1])
    load_x.start()
    load_c.start()
    loads = [
        pltpu.make_async_copy(wg_hbm, wg, load_sem.at[2]),
        pltpu.make_async_copy(wu_hbm, wu, load_sem.at[3]),
        pltpu.make_async_copy(wd_hbm, wd, load_sem.at[4]),
    ]
    for copy in loads:
        copy.start()

    r0 = routes_ref[0:1, :]
    r1 = routes_ref[1:2, :]
    ids = lax.broadcasted_iota(jnp.int32, (16, 128), 0)
    e0 = ids == r0
    e1 = ids == r1
    named = jnp.where(e0, 1.0, 0.0) + jnp.where(e1, 1.0, 0.0)
    before = jnp.where(
        lax.broadcasted_iota(jnp.int32, (128, 128), 0)
        < lax.broadcasted_iota(jnp.int32, (128, 128), 1),
        1.0, 0.0,
    ).astype(BF)
    earlier = mm(named.astype(BF), before, NN)
    t0 = r0.astype(F32) * 16.0 + jnp.sum(jnp.where(e0, earlier, 0.0), axis=0, keepdims=True)
    t1 = r1.astype(F32) * 16.0 + jnp.sum(jnp.where(e1, earlier, 0.0), axis=0, keepdims=True)
    place = lax.broadcasted_iota(jnp.int32, (256, 128), 0).astype(F32)
    p0 = place == t0
    p1 = place == t1
    perm_val = (jnp.where(p0, 1.0, 0.0) + jnp.where(p1, 1.0, 0.0)).astype(BF)
    perm[...] = perm_val
    w0 = weight_ref[0:1, :]
    w1 = weight_ref[1:2, :]
    w_slot = jnp.sum(jnp.where(p0, w0, 0.0) + jnp.where(p1, w1, 0.0), axis=1, keepdims=True)
    load_x.wait()
    sendbuf[0] = mm(perm_val, xq[...], NN).astype(BF)
    load_c.wait()
    sendbuf[1] = (w_slot * mm(perm_val, cq[...], NN)).astype(BF)

    pl.semaphore_wait(barrier, 19)

    m_own = g * 2 + c

    def rows_of(q):
        return pl.ds(pl.multiple_of(q * 16, 16), 16)

    for a in range(2):

        def push(k, _, a=a):
            q = lax.rem(me + k, 16)
            remote(
                sendbuf.at[a, rows_of(q)], xc.at[a, m_own, y, rows_of(me)],
                a2a_send.at[a, q], a2a_recv.at[a, me], holder(q),
            ).start()
            return 0

        lax.fori_loop(1, 16, push, 0)
    own = [
        pltpu.make_async_copy(
            sendbuf.at[a, rows_of(me)], xc.at[a, m_own, y, rows_of(me)], own_sem.at[a]
        )
        for a in range(2)
    ]
    own[0].start()
    own[1].start()

    def a2a_wait(a):
        def one(k, _):
            q = lax.rem(me + 16 - k, 16)
            remote(
                sendbuf.at[a, rows_of(q)], xc.at[a, m_own, y, rows_of(q)],
                a2a_send.at[a, q], a2a_recv.at[a, q], holder(q),
            ).wait_recv()
            return 0

        lax.fori_loop(1, 16, one, 0)
        own[a].wait()

    first, second = pl.ds(0, 128), pl.ds(128, 128)
    listed = [(g, y), (g, ym), (g, yp), (g, y2), (og, y), (og, ym), (og, yp), (og, y2)]

    def block(a, gg, cc, yy):
        return xc.at[a, gg * 2 + cc, yy]

    def ag_copy(a, kind, ref, dev):
        return remote(ref, ref, ag_send.at[a, kind], ag_recv.at[a, kind], dev)

    def ag_out(a, kind):
        if kind >= 8:
            gg, yy = listed[kind - 8]
            return ag_copy(a, kind, block(a, gg, c, yy), dev_s)
        ref, dev = (
            (block(a, g, c, y), dev_x),
            (block(a, g, c, y), dev_p),
            (block(a, g, c, y), dev_m),
            (block(a, g, c, ym).at[first], dev_p),
            (block(a, g, c, yp).at[second], dev_m),
            (block(a, og, c, y), dev_p),
            (block(a, og, c, y), dev_m),
            (block(a, g, c, y2), dev_x),
        )[kind]
        return ag_copy(a, kind, ref, dev)

    def ag_in(a, kind):
        if kind >= 8:
            gg, yy = listed[kind - 8]
            return ag_copy(a, kind, block(a, gg, oc, yy), dev_s)
        ref, dev = (
            (block(a, og, c, y), dev_x),
            (block(a, g, c, ym), dev_m),
            (block(a, g, c, yp), dev_p),
            (block(a, g, c, y2).at[first], dev_m),
            (block(a, g, c, y2).at[second], dev_p),
            (block(a, og, c, ym), dev_m),
            (block(a, og, c, yp), dev_p),
            (block(a, og, c, y2), dev_x),
        )[kind]
        return ag_copy(a, kind, ref, dev)

    def go(a, *kinds):
        for kind in kinds:
            ag_out(a, kind).start()

    def got(a, *kinds):
        for kind in kinds:
            ag_in(a, kind).wait_recv()

    a2a_wait(0)
    go(0, 0, 1, 2, 8)
    a2a_wait(1)
    go(1, 0, 1, 2, 8)
    got(0, 1)
    go(0, 3, 9)
    got(0, 2)
    go(0, 4, 10)
    got(1, 1)
    go(1, 3, 9)
    got(1, 2)
    go(1, 4, 10)
    got(0, 0)
    go(0, 5, 6, 12)
    got(1, 0)
    go(1, 5, 6, 12)
    got(0, 3, 4)
    go(0, 7, 11)
    got(1, 3, 4)
    go(1, 7, 11)

    for copy in loads:
        copy.wait()

    def forward(m):
        pre_g = jnp.zeros((256, 224), F32)
        pre_u = jnp.zeros((256, 224), F32)
        d_act = jnp.zeros((256, 224), F32)
        for q in range(4):
            span = slice(q * 512, q * 512 + 512)
            rows = xc[0, m, q]
            pre_g += mm(rows, wg[:, span], NT)
            pre_u += mm(rows, wu[:, span], NT)
            d_act += mm(xc[1, m, q], wd[:, span], NT)
        sig = jax.nn.sigmoid(pre_g)
        d_gate = (d_act * pre_u * swish_slope(pre_g, sig)).astype(BF)
        d_up = (d_act * pre_g * sig).astype(BF)
        act_t[m] = (pre_g * sig * pre_u).T.astype(BF)
        dg_t[m] = d_gate.T
        du_t[m] = d_up.T
        return d_gate, d_up

    def back(m, d_gate, d_up, yy):
        span = pl.ds(pl.multiple_of(yy * 512, 512), 512)
        part[m, yy] = (mm(d_gate, wg[:, span], NN) + mm(d_up, wu[:, span], NN)).astype(BF)

    def sib_copy(gg, j, yy):
        return remote(
            part.at[gg * 2 + oc, yy], sib_in.at[gg, yy],
            sb_send.at[gg, j], sb_recv.at[gg, j], dev_s,
        )

    order = (y2, yp, ym, y)

    def whole(gg, cc, sent):
        m = gg * 2 + cc
        d_gate, d_up = forward(m)
        for j, yy in enumerate(order):
            back(m, d_gate, d_up, yy)
            if sent:
                sib_copy(gg, j, yy).start()

    whole(g, c, False)
    got(0, 8, 9, 10, 11)
    got(1, 8, 9, 10, 11)
    got(0, 5)
    go(0, 13)
    got(0, 6)
    go(0, 14)
    got(0, 7)
    go(0, 15)
    whole(g, oc, True)
    got(1, 5)
    go(1, 13)
    got(1, 6)
    go(1, 14)
    got(1, 7)
    go(1, 15)
    whole(og, c, False)
    got(0, 12, 13, 14, 15)
    got(1, 12, 13, 14, 15)
    whole(og, oc, True)

    def pair_sum(gg, j):
        yy = order[j]
        sib_copy_in = remote(
            part.at[gg * 2 + oc, yy], sib_in.at[gg, yy],
            sb_send.at[gg, j], sb_recv.at[gg, j], dev_s,
        )
        sib_copy_in.wait_recv()
        m = gg * 2 + c
        part[m, yy] = (part[m, yy].astype(F32) + sib_in[gg, yy].astype(F32)).astype(BF)

    def rs_copy(kind, src, dst, dev):
        return remote(src, dst, rs_send.at[kind], rs_recv.at[kind], dev)

    m_g, m_o = g * 2 + c, og * 2 + c
    pair_sum(og, 0)
    send_a = rs_copy(0, part.at[m_o, y2], in_a, dev_x)
    send_a.start()
    pair_sum(og, 1)
    send_bp = rs_copy(1, part.at[m_o, yp], in_b.at[0], dev_p)
    send_bp.start()
    pair_sum(og, 2)
    send_bm = rs_copy(2, part.at[m_o, ym], in_b.at[1], dev_m)
    send_bm.start()
    for j in range(3):
        pair_sum(g, j)
    pair_sum(og, 3)
    pair_sum(g, 3)

    def weight_grad(i, source, a):
        def tile(q, _):
            acc = mm(source[0], xc[a, 0, q], NN)
            for m in range(1, 4):
                acc += mm(source[m], xc[a, m, q], NN)
            gout[i, :, pl.ds(pl.multiple_of(q * 512, 512), 512)] = acc.astype(BF)
            return 0

        lax.fori_loop(0, 4, tile, 0)

    weight_grad(0, dg_t, 0)
    outs = [
        pltpu.make_async_copy(gout.at[i], ref, out_sem.at[i])
        for i, ref in enumerate((gg_hbm, gu_hbm, gd_hbm))
    ]
    outs[0].start()
    weight_grad(1, du_t, 0)
    outs[1].start()
    send_a.wait_recv()
    part[m_g, y2] = (part[m_g, y2].astype(F32) + in_a[...].astype(F32)).astype(BF)
    send_cp = rs_copy(3, part.at[m_g, y2, first], in_c.at[0], dev_p)
    send_cm = rs_copy(4, part.at[m_g, y2, second], in_c.at[1], dev_m)
    send_cp.start()
    send_cm.start()
    send_bp.wait_recv()
    send_bm.wait_recv()
    part[m_o, y] = (
        part[m_o, y].astype(F32) + in_b[0].astype(F32) + in_b[1].astype(F32)
    ).astype(BF)
    send_d = rs_copy(5, part.at[m_o, y], in_d, dev_x)
    send_d.start()
    weight_grad(2, act_t, 1)
    outs[2].start()
    send_cp.wait_recv()
    part[m_g, yp, first] = (part[m_g, yp, first].astype(F32) + in_c[0].astype(F32)).astype(BF)
    send_ep = rs_copy(6, part.at[m_g, yp], in_e.at[0], dev_p)
    send_ep.start()
    send_cm.wait_recv()
    part[m_g, ym, second] = (part[m_g, ym, second].astype(F32) + in_c[1].astype(F32)).astype(BF)
    send_em = rs_copy(7, part.at[m_g, ym], in_e.at[1], dev_m)
    send_em.start()
    send_d.wait_recv()
    send_ep.wait_recv()
    send_em.wait_recv()
    total[...] = (
        part[m_g, y].astype(F32) + in_d[...].astype(F32)
        + in_e[0].astype(F32) + in_e[1].astype(F32)
    ).astype(BF)

    def push_back(k, _):
        q = lax.rem(me + k, 16)
        remote(
            total.at[rows_of(q)], ret.at[rows_of(me)], ret_send.at[q], ret_recv.at[me], holder(q)
        ).start()
        return 0

    lax.fori_loop(1, 16, push_back, 0)
    own_back = pltpu.make_async_copy(total.at[rows_of(me)], ret.at[rows_of(me)], own_sem.at[0])
    own_back.start()

    def wait_back(k, _):
        q = lax.rem(me + 16 - k, 16)
        remote(
            total.at[rows_of(q)], ret.at[rows_of(q)], ret_send.at[q], ret_recv.at[q], holder(q)
        ).wait_recv()
        return 0

    lax.fori_loop(1, 16, wait_back, 0)
    own_back.wait()
    moe = mm(perm[...], ret[...], TN)
    res_ref[y] = (cq[...].astype(F32) + moe).astype(BF)

    half0, half1 = pl.ds(0, 64), pl.ds(64, 64)

    def res_copy(kind, ref, dev):
        return remote(ref, ref, res_send.at[kind], res_recv.at[kind], dev)

    sends = [res_copy(0, res_ref.at[y], dev_p), res_copy(1, res_ref.at[y], dev_m)]
    sends[0].start()
    sends[1].start()
    res_copy(0, res_ref.at[ym], dev_m).wait_recv()
    sends.append(res_copy(2, res_ref.at[ym, half0], dev_p))
    sends[2].start()
    res_copy(1, res_ref.at[yp], dev_p).wait_recv()
    sends.append(res_copy(3, res_ref.at[yp, half1], dev_m))
    sends[3].start()
    res_copy(2, res_ref.at[y2, half0], dev_m).wait_recv()
    res_copy(3, res_ref.at[y2, half1], dev_p).wait_recv()

    for copy in outs:
        copy.wait()
    for a in range(2):

        def drain(k, _, a=a):
            q = lax.rem(me + k, 16)
            remote(
                sendbuf.at[a, rows_of(q)], xc.at[a, m_own, y, rows_of(me)],
                a2a_send.at[a, q], a2a_recv.at[a, me], holder(q),
            ).wait_send()
            return 0

        lax.fori_loop(1, 16, drain, 0)
        for kind in range(16):
            ag_out(a, kind).wait_send()

    def drain_back(k, _):
        q = lax.rem(me + k, 16)
        remote(
            total.at[rows_of(q)], ret.at[rows_of(me)], ret_send.at[q], ret_recv.at[me], holder(q)
        ).wait_send()
        return 0

    lax.fori_loop(1, 16, drain_back, 0)
    for gg in (g, og):
        for j, yy in enumerate(order):
            sib_copy(gg, j, yy).wait_send()
    for copy in (send_a, send_bp, send_bm, send_cp, send_cm, send_d, send_ep, send_em, *sends):
        copy.wait_send()


def expert_stage(routes_t, weight_t, moe_input, out_cot, wg, wu, wd):
    units, width = wg.shape
    vmem = pl.BlockSpec(memory_space=pltpu.VMEM)
    hbm = pl.BlockSpec(memory_space=pl.ANY)
    dma = pltpu.SemaphoreType.DMA
    grad = jax.ShapeDtypeStruct((units, width), BF)
    return pl.pallas_call(
        expert_kernel,
        out_shape=(grad, grad, grad, jax.ShapeDtypeStruct((4, 128, 512), BF)),
        in_specs=[vmem, vmem, hbm, hbm, hbm, hbm, hbm],
        out_specs=(hbm, hbm, hbm, vmem),
        scratch_shapes=[
            pltpu.VMEM((128, 512), BF),
            pltpu.VMEM((128, 512), BF),
            pltpu.VMEM((256, 128), BF),
            pltpu.VMEM((2, 256, 512), BF),
            pltpu.VMEM((2, 4, 4, 256, 512), BF),
            pltpu.VMEM((units, width), BF),
            pltpu.VMEM((units, width), BF),
            pltpu.VMEM((units, width), BF),
            pltpu.VMEM((4, units, 256), BF),
            pltpu.VMEM((4, units, 256), BF),
            pltpu.VMEM((4, units, 256), BF),
            pltpu.VMEM((3, units, width), BF),
            pltpu.VMEM((4, 4, 256, 512), BF),
            pltpu.VMEM((2, 4, 256, 512), BF),
            pltpu.VMEM((256, 512), BF),
            pltpu.VMEM((2, 256, 512), BF),
            pltpu.VMEM((2, 128, 512), BF),
            pltpu.VMEM((256, 512), BF),
            pltpu.VMEM((2, 256, 512), BF),
            pltpu.VMEM((256, 512), BF),
            pltpu.VMEM((256, 512), BF),
            dma((5,)), dma((3,)), dma((2,)),
            dma((2, 16)), dma((2, 16)), dma((2, 16)), dma((2, 16)),
            dma((2, 4)), dma((2, 4)), dma((8,)), dma((8,)),
            dma((16,)), dma((16,)), dma((4,)), dma((4,)),
        ],
        compiler_params=pltpu.CompilerParams(
            collective_id=0, has_side_effects=True, vmem_limit_bytes=60 * 1024 * 1024
        ),
        name="expert_stage",
    )(routes_t, weight_t, moe_input, out_cot, wg, wu, wd)


def in_blocks(array, dim, size):
    lengths = array.shape
    blocks = array.reshape(*lengths[:dim], size, lengths[dim] // size, *lengths[dim + 1 :])
    return jnp.moveaxis(blocks, dim, 0)


def sum_at_owner(array, axis, dim):
    size = lax.axis_size(axis)
    blocks = lax.all_to_all(in_blocks(array, dim, size), axis, 0, 0, tiled=True)
    return jnp.sum(blocks.astype(jnp.float32), axis=0)


def from_behind(block, axis, distance):
    devices = range(lax.axis_size(axis))
    route = [(i - distance, i) for i in devices if i - distance in devices]
    return lax.ppermute(block, axis, route)


def local(
    moe_input,
    out_cotangent,
    routes,
    route_weight,
    w_gate,
    w_up,
    w_down,
    out_proj,
    conv_out,
    glu_value,
    glu_gate,
    taps,
    norm_gain,
):
    grad_gate, grad_up, grad_down, resid = expert_stage(
        routes.T, route_weight.T, moe_input, out_cotangent,
        w_gate[0].T, w_up[0].T, w_down[0],
    )
    resid_grad = jnp.swapaxes(resid, 1, 2).reshape(2048, 128)
    conv_vals = conv_out.astype(jnp.float32)
    total_sum, square_sum = lax.psum(
        (jnp.sum(conv_vals, axis=1), jnp.sum(conv_vals * conv_vals, axis=1)), "tp"
    )
    mean = total_sum[:, None] / DB
    rstd = lax.rsqrt(square_sum[:, None] / DB - mean * mean + 1e-05)
    normed = (conv_vals - mean) * rstd
    zpre = normed * norm_gain[None, :]
    zsig = jax.nn.sigmoid(zpre)
    mixed = (zpre * zsig).astype(jnp.bfloat16)
    grad_proj = sum_at_owner(
        jnp.dot(resid_grad, mixed, preferred_element_type=jnp.float32).astype(jnp.bfloat16), "sp", 0
    )
    d_mixed = lax.dot_general(
        resid_grad, out_proj, (((0,), (0,)), ((), ())), preferred_element_type=jnp.float32
    )
    d_norm = d_mixed * swish_slope(zpre, zsig) * norm_gain[None, :]
    first_sum, second_sum = lax.psum(
        (jnp.sum(d_norm, axis=1), jnp.sum(d_norm * normed, axis=1)), "tp"
    )
    conv_grad = (
        rstd * (d_norm - first_sum[:, None] / DB - normed * second_sum[:, None] / DB)
    ).astype(jnp.bfloat16)
    later_rows = from_behind(conv_grad[: WIDTH - 1], "sp", -1)
    extended = jnp.concatenate([conv_grad, later_rows], axis=0).astype(jnp.float32)
    unit_grad = lax.conv_general_dilated(
        extended[None],
        taps[:, None, :],
        (1,),
        "VALID",
        dimension_numbers=("NWC", "WIO", "NWC"),
        feature_group_count=taps.shape[1],
        precision=lax.Precision.HIGHEST,
    )[0]
    gate_sig_in = jax.nn.sigmoid(glu_gate.astype(jnp.float32))
    grad_glu_value = (unit_grad * gate_sig_in).astype(jnp.bfloat16)
    grad_glu_gate = (
        unit_grad * glu_value.astype(jnp.float32) * gate_sig_in * (1.0 - gate_sig_in)
    ).astype(jnp.bfloat16)
    return (grad_gate.T[None], grad_up.T[None], grad_down[None], grad_proj, grad_glu_value, grad_glu_gate)


def solution(mesh):
    in_specs = (
        P("sp", None),
        P("sp", None),
        P("sp", None),
        P("sp", None),
        P("sp", None, "tp"),
        P("sp", None, "tp"),
        P("sp", "tp", None),
        P(None, "tp"),
        P("sp", "tp"),
        P("sp", "tp"),
        P("sp", "tp"),
        P(None, "tp"),
        P("tp"),
    )
    out_specs = (
        P("sp", None, "tp"),
        P("sp", None, "tp"),
        P("sp", "tp", None),
        P("sp", "tp"),
        P("sp", "tp"),
        P("sp", "tp"),
    )
    return jax.shard_map(local, mesh=mesh, in_specs=in_specs, out_specs=out_specs, check_vma=False)
```

time: 380 us -> 150 us (0.39)
  the two profiles are of different devices: /device:TPU:16 before, /device:TPU:1 now
where the time goes in v1:
time: 150 us
  Pallas kernels  91.9 us (61%)
  starting transfers between devices  16.9 us (11%)
  waiting for transfers between devices  15.2 us (10%)
  blocking collectives  14.2 us (9%)
  local copies, waits for them, and re-layouts  5.65 us (4%)
  other arithmetic  2.7 us (2%)
  matrix products  2.46 us (2%)
    pallas_call x1, Pallas kernels, expert_stage(): pl.pallas_call(expert_kernel, out_shape=(grad, grad, grad, jax.ShapeDtype...  91.9 us
    all_to_all x1, starting transfers between devices, sum_at_owner(): blocks = lax.all_to_all(in_blocks(array, dim, size), axis, 0, 0, tiled=True)  13.1 us
    all_to_all x1, waiting for transfers between devices, sum_at_owner(): blocks = lax.all_to_all(in_blocks(array, dim, size), axis, 0, 0, tiled=True)  12.2 us
    psum x1, blocking collectives, local(): lax.psum((jnp.sum(conv_vals, axis=1), jnp.sum(conv_vals * conv_vals, axis...  7.29 us
    psum x1, blocking collectives, local(): lax.psum((jnp.sum(d_norm, axis=1), jnp.sum(d_norm * normed, axis=1)), 'tp')  6.93 us
    unnamed x21, local copies, waits for them, and re-layouts  4.31 us
    ppermute x1, starting transfers between devices, from_behind(): return lax.ppermute(block, axis, route)  3.79 us
    ppermute x1, waiting for transfers between devices, from_behind(): return lax.ppermute(block, axis, route)  3.01 us
  transfers between devices with their start and end apart: 2, of which 2 were waited for; matrix products, arithmetic and copies ran while one was open for 1% of the time, Pallas kernels for 0%

profile of v1, /device:TPU:1, one launch (start us, length us, event | category | flops | bytes accessed | tf_op | source)
XLA Modules:
  0.0 149.8 jit_solution(4029912251004263695)
XLA Ops:
  0.6 0.0 copy-start
  0.6 1.0 convert_reduce_fusion.1
  1.7 91.9 %expert_stage.1 = (bf16[224,2048]{1,0:T(8,128)(2,1)}, bf16[224,2048]{1,0:T(8,128)(2,1)}, bf16[224,2048]{1,0:T(8,128)(2,1)}, bf16[4,128,512]{2,1,0:T(8,128)(2,1)}) custom-call(s32[2,128]{1,0:T(2,128)} %bitcast.45, f32[2,128]{1,0:T(2,128)} %bitcast.46, bf16[128,2048]{1,0:T(8,128)(2,1)} %x_hbm.1, bf16[128,2048]{1,0:T(8,128)(2,1)} %cot_hbm.1, ...), custom_call_target="tpu_custom_call" | custom-call | tf_op jit(solution)/shard_map/expert_stage/pallas_call | solution.py:439
  93.6 0.0 copy-start.4
  93.6 0.0 copy-start.7
  93.6 1.3 copy.21
  95.0 7.3 %all-reduce.1 = (f32[128]{0:T(128)S(1)}, f32[128]{0:T(128)S(1)}) all-reduce(f32[128]{0:T(128)S(1)} %get-tuple-element.17, f32[128]{0:T(128)S(1)} %get-tuple-element.16), channel_id=1, replica_groups=mesh['sp'=64,'tp'=4] {'tp'}, use_global_device_ids=true, to_apply=%region_3.0 | all-reduce | flops 256 | bytes 2048 | tf_op jit(solution)/shard_map/psum | solution.py:517
  102.3 0.0 copy-done.4
  102.3 0.0 copy-done.7
  102.3 1.5 %convolution_convert_fusion = bf16[2048,256]{1,0:T(8,128)(2,1)} fusion(bf16[2048,128]{1,0:T(8,128)(2,1)S(1)} %bitcast.36, bf16[128,256]{1,0:T(8,128)(2,1)S(1)} %copy-done.4, f32[256]{0:T(256)S(1)} %copy-done.7, f32[128]{0:T(128)S(1)} %get-tuple-element.25, f32[128]{0:T(128)S(1)} %get-tuple-element.24), kind=kOutput, calls=%fused_computation | convolution fusion | flops 135036928 | bytes 1640448 | tf_op jit(solution)/shard_map/dot_general | solution.py:527
  103.8 13.1 %all-to-all-start = ((bf16[64,32,256]{2,1,0:T(8,128)(2,1)}), bf16[64,32,256]{2,1,0:T(8,128)(2,1)S(1)}, u32[]{:S(2)}, u32[]{:S(2)}) async-start(bf16[64,32,256]{2,1,0:T(8,128)(2,1)} %bitcast.14), calls=%async_computation | async-start | bytes 2097152 | tf_op jit(solution)/shard_map/all_to_all | solution.py:486
  117.0 0.0 copy-done
  117.0 0.0 copy-start.8
  117.0 0.4 fusion.33
  117.4 6.9 %all-reduce = (f32[128]{0:T(128)S(1)}, f32[128]{0:T(128)S(1)}) all-reduce(f32[128]{0:T(128)S(1)} %get-tuple-element.15, f32[128]{0:T(128)S(1)} %get-tuple-element.14), channel_id=1, replica_groups=mesh['sp'=64,'tp'=4] {'tp'}, use_global_device_ids=true, to_apply=%region_8.0 | all-reduce | flops 256 | bytes 2048 | tf_op jit(solution)/shard_map/psum | solution.py:533
  124.4 0.1 fusion.20
  124.5 3.8 %collective-permute-start = (bf16[30,256]{1,0:T(8,128)(2,1)S(1)}, bf16[30,256]{1,0:T(8,128)(2,1)S(1)}, u32[]{:S(2)}, u32[]{:S(2)}) collective-permute-start(bf16[30,256]{1,0:T(8,128)(2,1)S(1)} %slice.4), channel_id=1, source_target_pairs={{4,0},{8,4},{12,8},{16,12},{20,16},{24,20},{28,24},{32,28},{36,32}... | collective-permute-start | bytes 46088 | tf_op jit(solution)/shard_map/ppermute | solution.py:493
  128.3 3.0 %collective-permute-done = bf16[30,256]{1,0:T(8,128)(2,1)S(1)} collective-permute-done((bf16[30,256]{1,0:T(8,128)(2,1)S(1)}, bf16[30,256]{1,0:T(8,128)(2,1)S(1)}, u32[]{:S(2)}, u32[]{:S(2)}) %collective-permute-start) | collective-permute-done | bytes 15392 | tf_op jit(solution)/shard_map/ppermute | solution.py:493
  131.3 0.0 copy-done.8
  131.3 0.0 copy-start.5
  131.3 0.0 copy-start.6
  131.4 0.5 fusion.1
  131.9 0.3 copy-done.5
  132.2 0.0 copy-done.6
  132.2 0.0 copy-start.3
  132.2 0.7 fusion.25
  132.9 12.2 %all-to-all-done = bf16[64,32,256]{2,1,0:T(8,128)(2,1)S(1)} async-done(((bf16[64,32,256]{2,1,0:T(8,128)(2,1)}), bf16[64,32,256]{2,1,0:T(8,128)(2,1)S(1)}, u32[]{:S(2)}, u32[]{:S(2)}) %all-to-all-start) | async-done | bytes 1048608 | tf_op jit(solution)/shard_map/all_to_all | solution.py:486
  145.1 0.8 convert_reduce_fusion
  145.9 0.0 copy-start.2
  145.9 0.0 copy-done.3
  145.9 0.9 copy.34
  146.8 0.6 copy-done.2
  147.4 0.0 copy-start.1
  147.4 0.9 copy.35
  148.3 0.6 copy-done.1
  148.9 0.9 copy.36
  (4 shorter events, 0.0 us)
Async XLA Ops:
  0.6 116.3 %copy-start = (bf16[2048,256]{1,0:T(8,128)(2,1)S(1)}, bf16[2048,256]{1,0:T(8,128)(2,1)}, u32[]{:S(2)}) copy-start(bf16[2048,256]{1,0:T(8,128)(2,1)} %param.20) | copy-start | bytes 3145732
  93.6 8.7 %copy-start.4 = (bf16[128,256]{1,0:T(8,128)(2,1)S(1)}, bf16[128,256]{1,0:T(8,128)(2,1)}, u32[]{:S(2)}) copy-start(bf16[128,256]{1,0:T(8,128)(2,1)} %param.21) | copy-start | bytes 196612
  93.6 8.7 %copy-start.7 = (f32[256]{0:T(256)S(1)}, f32[256]{0:T(256)}, u32[]{:S(2)}) copy-start(f32[256]{0:T(256)} %param.25) | copy-start | bytes 3076
  103.8 41.3 %all-to-all-start = ((bf16[64,32,256]{2,1,0:T(8,128)(2,1)}), bf16[64,32,256]{2,1,0:T(8,128)(2,1)S(1)}, u32[]{:S(2)}, u32[]{:S(2)}) async-start(bf16[64,32,256]{2,1,0:T(8,128)(2,1)} %bitcast.14), calls=%async_computation | async-start | bytes 2097152 | tf_op jit(solution)/shard_map/all_to_all | solution.py:486
  117.0 14.4 %copy-start.8 = (f32[31,256]{1,0:T(8,128)S(1)}, f32[31,256]{1,0:T(8,128)}, u32[]{:S(2)}) copy-start(f32[31,256]{1,0:T(8,128)} %param.24) | copy-start | bytes 95236
  124.5 6.8 %collective-permute-start = (bf16[30,256]{1,0:T(8,128)(2,1)S(1)}, bf16[30,256]{1,0:T(8,128)(2,1)S(1)}, u32[]{:S(2)}, u32[]{:S(2)}) collective-permute-start(bf16[30,256]{1,0:T(8,128)(2,1)S(1)} %slice.4), channel_id=1, source_target_pairs={{4,0},{8,4},{12,8},{16,12},{20,16},{24,20},{28,24},{32,28},{36,32}... | collective-permute-start | bytes 46088 | tf_op jit(solution)/shard_map/ppermute | solution.py:493
  131.3 0.8 copy-start.5
  131.3 0.9 copy-start.6
  132.2 13.7 %copy-start.3 = (bf16[224,2048]{1,0:T(8,128)(2,1)S(1)}, bf16[224,2048]{1,0:T(8,128)(2,1)}, u32[]{:S(2)}) copy-start(bf16[224,2048]{1,0:T(8,128)(2,1)} %get-tuple-element.10) | copy-start | bytes 2752516
  145.9 1.5 %copy-start.2 = (bf16[224,2048]{1,0:T(8,128)(2,1)S(1)}, bf16[224,2048]{1,0:T(8,128)(2,1)}, u32[]{:S(2)}) copy-start(bf16[224,2048]{1,0:T(8,128)(2,1)} %get-tuple-element.11) | copy-start | bytes 2752516
  147.4 1.5 %copy-start.1 = (bf16[224,2048]{1,0:T(8,128)(2,1)S(1)}, bf16[224,2048]{1,0:T(8,128)(2,1)}, u32[]{:S(2)}) copy-start(bf16[224,2048]{1,0:T(8,128)(2,1)} %get-tuple-element.12) | copy-start | bytes 2752516

commit v2 on v1

--- a/solution.py
+++ b/solution.py
@@ -7,7 +7,6 @@
 
 DB = 1024
 WIDTH = 31
-SPAN = 4
 MESH = pl.DeviceIdType.MESH
 BF = jnp.bfloat16
 F32 = jnp.float32
@@ -24,13 +23,17 @@
     return sig * (1.0 + pre * (1.0 - sig))
 
 
-def expert_kernel(
-    routes_ref, weight_ref, x_hbm, cot_hbm, wg_hbm, wu_hbm, wd_hbm,
-    gg_hbm, gu_hbm, gd_hbm, res_ref,
+def backward_kernel(
+    routes_ref, weight_ref, conv_ref, value_ref, gate_ref, taps_ref, gain_ref,
+    x_hbm, cot_hbm, wg_hbm, wu_hbm, wd_hbm, proj_hbm,
+    gg_hbm, gu_hbm, gd_hbm, gp_ref, gv_ref, gt_ref,
     xq, cq, perm, sendbuf, xc, wg, wu, wd, act_t, dg_t, du_t, gout,
     part, sib_in, in_a, in_b, in_c, in_d, in_e, total, ret,
+    res_ref, proj, normed, slope, mixed, scale, st_out, st_in, ext, halo_out, halo_in,
+    gp, gp_sib, gp_x, gp_row, gp_z,
     load_sem, out_sem, own_sem, a2a_send, a2a_recv, ag_send, ag_recv,
     sb_send, sb_recv, rs_send, rs_recv, ret_send, ret_recv, res_send, res_recv,
+    st_send, st_recv, halo_sem, gs_send, gs_recv, gx_send, gx_recv, gz_send, gz_recv,
 ):
     sp = lax.axis_index("sp")
     y = lax.axis_index("tp")
@@ -54,6 +57,16 @@
     dev_s = (z * 8 + x * 2 + oc, y)
     dev_p = (sp, yp)
     dev_m = (sp, ym)
+    dev_2 = (sp, y2)
+    dev_prev = (lax.rem(sp + 63, 64), y)
+    dev_next = (lax.rem(sp + 1, 64), y)
+    others_x = (xh * 2 + 1 - xl, (1 - xh) * 2 + xl, (1 - xh) * 2 + 1 - xl)
+
+    def at_x(xx):
+        return (z * 8 + xx * 2 + c, y)
+
+    def at_z(zz):
+        return (zz * 8 + x * 2 + c, y)
 
     def remote(src, dst, ss, rs, dev):
         return pltpu.make_async_remote_copy(
@@ -68,7 +81,10 @@
         return 0
 
     lax.fori_loop(1, 16, greet, 0)
-    for dev in (dev_x, dev_s, dev_p, dev_m):
+    greeted = (
+        dev_x, dev_s, dev_p, dev_m, dev_2, at_x(others_x[1]), at_x(others_x[2]), dev_prev, dev_next
+    )
+    for dev in greeted:
         pl.semaphore_signal(barrier, inc=1, device_id=dev, device_id_type=MESH)
 
     cols = pl.ds(pl.multiple_of(y * 512, 512), 512)
@@ -83,6 +99,8 @@
     ]
     for copy in loads:
         copy.start()
+    load_proj = pltpu.make_async_copy(proj_hbm, proj, load_sem.at[5])
+    load_proj.start()
 
     r0 = routes_ref[0:1, :]
     r1 = routes_ref[1:2, :]
@@ -111,7 +129,7 @@
     load_c.wait()
     sendbuf[1] = (w_slot * mm(perm_val, cq[...], NN)).astype(BF)
 
-    pl.semaphore_wait(barrier, 19)
+    pl.semaphore_wait(barrier, 24)
 
     m_own = g * 2 + c
 
@@ -149,6 +167,34 @@
 
         lax.fori_loop(1, 16, one, 0)
         own[a].wait()
+
+    lane = lax.broadcasted_iota(jnp.int32, (128, 128), 1)
+
+    def sums_out(phase, one, two):
+        cols2 = jnp.where(lane == 0, one, 0.0) + jnp.where(lane == 1, two, 0.0)
+        st_out[phase] = cols2.T[0:8, :]
+        return [
+            remote(
+                st_out.at[phase], st_in.at[phase, j], st_send.at[phase, j], st_recv.at[phase, j], dev
+            )
+            for j, dev in enumerate((dev_p, dev_m, dev_2))
+        ]
+
+    def sums_in(phase, copies):
+        for copy in copies:
+            copy.wait_recv()
+        tot = (st_out[phase] + st_in[phase, 2]) + (st_in[phase, 0] + st_in[phase, 1])
+        tall = jnp.concatenate([tot, jnp.zeros((120, 128), F32)], axis=0).T
+        return tall[:, 0:1], tall[:, 1:2]
+
+    conv_vals = conv_ref[...].astype(F32)
+    stats = sums_out(
+        0,
+        jnp.sum(conv_vals, axis=1, keepdims=True),
+        jnp.sum(conv_vals * conv_vals, axis=1, keepdims=True),
+    )
+    for copy in stats:
+        copy.start()
 
     first, second = pl.ds(0, 128), pl.ds(128, 128)
     listed = [(g, y), (g, ym), (g, yp), (g, y2), (og, y), (og, ym), (og, yp), (og, y2)]
@@ -215,6 +261,16 @@
     go(0, 5, 6, 12)
     got(1, 0)
     go(1, 5, 6, 12)
+    sum1, sum2 = sums_in(0, stats)
+    mean = sum1 / DB
+    rstd = lax.rsqrt(sum2 / DB - mean * mean + 1e-05)
+    norm_val = (conv_ref[...].astype(F32) - mean) * rstd
+    zpre = norm_val * gain_ref[...]
+    zsig = jax.nn.sigmoid(zpre)
+    normed[...] = norm_val
+    mixed[...] = (zpre * zsig).astype(BF)
+    slope[...] = swish_slope(zpre, zsig) * gain_ref[...]
+    scale[...] = jnp.broadcast_to(rstd, (128, 256))
     got(0, 3, 4)
     go(0, 7, 11)
     got(1, 3, 4)
@@ -390,14 +446,110 @@
     sends = [res_copy(0, res_ref.at[y], dev_p), res_copy(1, res_ref.at[y], dev_m)]
     sends[0].start()
     sends[1].start()
+    load_proj.wait()
+
+    def gp_copy(q, j):
+        pair = pl.ds(q * 2, 2)
+        return remote(
+            gp.at[oc, :, pair], gp_sib.at[:, pair], gs_send.at[j], gs_recv.at[j], dev_s
+        )
+
+    def proj_terms(q, j):
+        feats = res_ref[q]
+        term = mm(feats, mixed[...], TN)
+        for i in range(8):
+            for cc in range(2):
+                gp[cc, i % 4, q * 2 + i // 4] = term[i * 64 + cc * 32 : i * 64 + cc * 32 + 32].astype(BF)
+        gp_copy(q, j).start()
+        return mm(feats, proj[pl.ds(pl.multiple_of(q * 512, 512), 512), :], NN)
+
+    d_mixed = proj_terms(y, 0)
     res_copy(0, res_ref.at[ym], dev_m).wait_recv()
     sends.append(res_copy(2, res_ref.at[ym, half0], dev_p))
     sends[2].start()
     res_copy(1, res_ref.at[yp], dev_p).wait_recv()
     sends.append(res_copy(3, res_ref.at[yp, half1], dev_m))
     sends[3].start()
+    d_mixed += proj_terms(ym, 1)
+    d_mixed += proj_terms(yp, 2)
     res_copy(2, res_ref.at[y2, half0], dev_m).wait_recv()
     res_copy(3, res_ref.at[y2, half1], dev_p).wait_recv()
+    d_mixed += proj_terms(y2, 3)
+    d_norm = d_mixed * slope[...]
+    norm_val = normed[...]
+    stats2 = sums_out(
+        1,
+        jnp.sum(d_norm, axis=1, keepdims=True),
+        jnp.sum(d_norm * norm_val, axis=1, keepdims=True),
+    )
+    for copy in stats2:
+        copy.start()
+
+    for j, q in enumerate((y, ym, yp, y2)):
+        gp_copy(q, j).wait_recv()
+
+    def pair_rows(xx):
+        gp[c, xx] = (gp[c, xx].astype(F32) + gp_sib[xx].astype(F32)).astype(BF)
+
+    def gx_copy(j):
+        return remote(
+            gp.at[c, others_x[j]], gp_x.at[j], gx_send.at[j], gx_recv.at[j], at_x(others_x[j])
+        )
+
+    for j in (1, 2, 0):
+        pair_rows(others_x[j])
+        gx_copy(j).start()
+    pair_rows(x)
+
+    first_sum, second_sum = sums_in(1, stats2)
+    conv_grad = (
+        scale[...] * (d_norm - first_sum / DB - norm_val * (second_sum / DB))
+    ).astype(BF)
+    halo_out[...] = conv_grad[0:32]
+    halo = remote(halo_out, halo_in, halo_sem.at[0], halo_sem.at[1], dev_prev)
+    halo.start()
+    ext[0:128, :] = conv_grad.astype(F32)
+
+    def correlate(start, count):
+        acc = jnp.zeros((count, 256), F32)
+        for k in range(WIDTH):
+            acc += ext[start + k : start + k + count, :] * taps_ref[k : k + 1, :]
+        return acc
+
+    def glu_grads(start, count, unit_grad):
+        span = slice(start, start + count)
+        sig = jax.nn.sigmoid(gate_ref[span, :].astype(F32))
+        gv_ref[span, :] = (unit_grad * sig).astype(BF)
+        gt_ref[span, :] = (
+            unit_grad * value_ref[span, :].astype(F32) * sig * (1.0 - sig)
+        ).astype(BF)
+
+    glu_grads(0, 64, correlate(0, 64))
+    glu_grads(64, 32, correlate(64, 32))
+
+    for j in range(3):
+        gx_copy(j).wait_recv()
+
+    def gz_copy(k):
+        zz = lax.rem(z + k, 8)
+        return remote(gp_row.at[zz], gp_z.at[k], gz_send.at[k], gz_recv.at[k], at_z(zz))
+
+    gp_row[...] = (
+        (gp[c, x].astype(F32) + gp_x[0].astype(F32)) + (gp_x[1].astype(F32) + gp_x[2].astype(F32))
+    ).astype(BF)
+    for k in (4, 3, 5, 2, 6, 1, 7):
+        gz_copy(k).start()
+
+    halo.wait_recv()
+    keep = jnp.where(sp < 63, 1.0, 0.0)
+    ext[128:160, :] = halo_in[...].astype(F32) * keep
+    glu_grads(96, 32, correlate(96, 32))
+
+    rows_sum = gp_row[z].astype(F32)
+    for k in range(1, 8):
+        gz_copy(k).wait_recv()
+        rows_sum += gp_z[k].astype(F32)
+    gp_ref[...] = rows_sum
 
     for copy in outs:
         copy.wait()
@@ -428,19 +580,43 @@
             sib_copy(gg, j, yy).wait_send()
     for copy in (send_a, send_bp, send_bm, send_cp, send_cm, send_d, send_ep, send_em, *sends):
         copy.wait_send()
-
-
-def expert_stage(routes_t, weight_t, moe_input, out_cot, wg, wu, wd):
-    units, width = wg.shape
+    for copy in (*stats, *stats2, halo):
+        copy.wait_send()
+    for j, q in enumerate((y, ym, yp, y2)):
+        gp_copy(q, j).wait_send()
+    for j in range(3):
+        gx_copy(j).wait_send()
+    for k in range(1, 8):
+        gz_copy(k).wait_send()
+
+
+def local(
+    moe_input,
+    out_cotangent,
+    routes,
+    route_weight,
+    w_gate,
+    w_up,
+    w_down,
+    out_proj,
+    conv_out,
+    glu_value,
+    glu_gate,
+    taps,
+    norm_gain,
+):
+    units, width = w_down.shape[1:]
+    tokens, channels = conv_out.shape
     vmem = pl.BlockSpec(memory_space=pltpu.VMEM)
     hbm = pl.BlockSpec(memory_space=pl.ANY)
     dma = pltpu.SemaphoreType.DMA
     grad = jax.ShapeDtypeStruct((units, width), BF)
-    return pl.pallas_call(
-        expert_kernel,
-        out_shape=(grad, grad, grad, jax.ShapeDtypeStruct((4, 128, 512), BF)),
-        in_specs=[vmem, vmem, hbm, hbm, hbm, hbm, hbm],
-        out_specs=(hbm, hbm, hbm, vmem),
+    glu = jax.ShapeDtypeStruct((tokens, channels), BF)
+    gg, gu, gd, gp, gv, gt = pl.pallas_call(
+        backward_kernel,
+        out_shape=(grad, grad, grad, jax.ShapeDtypeStruct((32, channels), F32), glu, glu),
+        in_specs=[vmem] * 7 + [hbm] * 6,
+        out_specs=(hbm, hbm, hbm, vmem, vmem, vmem),
         scratch_shapes=[
             pltpu.VMEM((128, 512), BF),
             pltpu.VMEM((128, 512), BF),
@@ -463,96 +639,38 @@
             pltpu.VMEM((2, 256, 512), BF),
             pltpu.VMEM((256, 512), BF),
             pltpu.VMEM((256, 512), BF),
-            dma((5,)), dma((3,)), dma((2,)),
+            pltpu.VMEM((4, 128, 512), BF),
+            pltpu.VMEM((width, 256), BF),
+            pltpu.VMEM((128, 256), F32),
+            pltpu.VMEM((128, 256), F32),
+            pltpu.VMEM((128, 256), BF),
+            pltpu.VMEM((128, 256), F32),
+            pltpu.VMEM((2, 8, 128), F32),
+            pltpu.VMEM((2, 3, 8, 128), F32),
+            pltpu.VMEM((160, 256), F32),
+            pltpu.VMEM((32, 256), BF),
+            pltpu.VMEM((32, 256), BF),
+            pltpu.VMEM((2, 4, 8, 32, 256), BF),
+            pltpu.VMEM((4, 8, 32, 256), BF),
+            pltpu.VMEM((3, 8, 32, 256), BF),
+            pltpu.VMEM((8, 32, 256), BF),
+            pltpu.VMEM((8, 32, 256), BF),
+            dma((6,)), dma((3,)), dma((2,)),
             dma((2, 16)), dma((2, 16)), dma((2, 16)), dma((2, 16)),
             dma((2, 4)), dma((2, 4)), dma((8,)), dma((8,)),
             dma((16,)), dma((16,)), dma((4,)), dma((4,)),
+            dma((2, 3)), dma((2, 3)), dma((2,)),
+            dma((4,)), dma((4,)), dma((3,)), dma((3,)), dma((8,)), dma((8,)),
         ],
         compiler_params=pltpu.CompilerParams(
             collective_id=0, has_side_effects=True, vmem_limit_bytes=60 * 1024 * 1024
         ),
-        name="expert_stage",
-    )(routes_t, weight_t, moe_input, out_cot, wg, wu, wd)
-
-
-def in_blocks(array, dim, size):
-    lengths = array.shape
-    blocks = array.reshape(*lengths[:dim], size, lengths[dim] // size, *lengths[dim + 1 :])
-    return jnp.moveaxis(blocks, dim, 0)
-
-
-def sum_at_owner(array, axis, dim):
-    size = lax.axis_size(axis)
-    blocks = lax.all_to_all(in_blocks(array, dim, size), axis, 0, 0, tiled=True)
-    return jnp.sum(blocks.astype(jnp.float32), axis=0)
-
-
-def from_behind(block, axis, distance):
-    devices = range(lax.axis_size(axis))
-    route = [(i - distance, i) for i in devices if i - distance in devices]
-    return lax.ppermute(block, axis, route)
-
-
-def local(
-    moe_input,
-    out_cotangent,
-    routes,
-    route_weight,
-    w_gate,
-    w_up,
-    w_down,
-    out_proj,
-    conv_out,
-    glu_value,
-    glu_gate,
-    taps,
-    norm_gain,
-):
-    grad_gate, grad_up, grad_down, resid = expert_stage(
-        routes.T, route_weight.T, moe_input, out_cotangent,
-        w_gate[0].T, w_up[0].T, w_down[0],
+        name="backward",
+    )(
+        routes.T, route_weight.T, conv_out, glu_value, glu_gate, taps, norm_gain[None, :],
+        moe_input, out_cotangent, w_gate[0].T, w_up[0].T, w_down[0], out_proj,
     )
-    resid_grad = jnp.swapaxes(resid, 1, 2).reshape(2048, 128)
-    conv_vals = conv_out.astype(jnp.float32)
-    total_sum, square_sum = lax.psum(
-        (jnp.sum(conv_vals, axis=1), jnp.sum(conv_vals * conv_vals, axis=1)), "tp"
-    )
-    mean = total_sum[:, None] / DB
-    rstd = lax.rsqrt(square_sum[:, None] / DB - mean * mean + 1e-05)
-    normed = (conv_vals - mean) * rstd
-    zpre = normed * norm_gain[None, :]
-    zsig = jax.nn.sigmoid(zpre)
-    mixed = (zpre * zsig).astype(jnp.bfloat16)
-    grad_proj = sum_at_owner(
-        jnp.dot(resid_grad, mixed, preferred_element_type=jnp.float32).astype(jnp.bfloat16), "sp", 0
-    )
-    d_mixed = lax.dot_general(
-        resid_grad, out_proj, (((0,), (0,)), ((), ())), preferred_element_type=jnp.float32
-    )
-    d_norm = d_mixed * swish_slope(zpre, zsig) * norm_gain[None, :]
-    first_sum, second_sum = lax.psum(
-        (jnp.sum(d_norm, axis=1), jnp.sum(d_norm * normed, axis=1)), "tp"
-    )
-    conv_grad = (
-        rstd * (d_norm - first_sum[:, None] / DB - normed * second_sum[:, None] / DB)
-    ).astype(jnp.bfloat16)
-    later_rows = from_behind(conv_grad[: WIDTH - 1], "sp", -1)
-    extended = jnp.concatenate([conv_grad, later_rows], axis=0).astype(jnp.float32)
-    unit_grad = lax.conv_general_dilated(
-        extended[None],
-        taps[:, None, :],
-        (1,),
-        "VALID",
-        dimension_numbers=("NWC", "WIO", "NWC"),
-        feature_group_count=taps.shape[1],
-        precision=lax.Precision.HIGHEST,
-    )[0]
-    gate_sig_in = jax.nn.sigmoid(glu_gate.astype(jnp.float32))
-    grad_glu_value = (unit_grad * gate_sig_in).astype(jnp.bfloat16)
-    grad_glu_gate = (
-        unit_grad * glu_value.astype(jnp.float32) * gate_sig_in * (1.0 - gate_sig_in)
-    ).astype(jnp.bfloat16)
-    return (grad_gate.T[None], grad_up.T[None], grad_down[None], grad_proj, grad_glu_value, grad_glu_gate)
+    return (gg.T[None], gu.T[None], gd[None], gp, gv, gt)
 
 
 def solution(mesh):

time: 150 us -> 120 us (0.80)
  Pallas kernels: 91.9 us -> 112 us
  starting transfers between devices: 16.9 us -> 0 us
  waiting for transfers between devices: 15.2 us -> 0 us
  blocking collectives: 14.2 us -> 0 us
  other arithmetic: 2.7 us -> 0 us
  matrix products: 2.46 us -> 0 us
    pallas_call x1, Pallas kernels: 91.9 us -> 112 us  [local(): pl.pallas_call(backward_kernel, out_shape=(grad, grad, grad, jax.ShapeDty...]
    psum x2 -> x0, blocking collectives: 14.2 us -> none  [the longest x1 7.29 us: local(): lax.psum((jnp.sum(conv_vals, axis=1), jnp.sum(conv_vals * conv_vals, axis...]
    all_to_all x1 -> x0, starting transfers between devices: 13.1 us -> none  [sum_at_owner(): blocks = lax.all_to_all(in_blocks(array, dim, size), axis, 0, 0, tiled=True)]
    all_to_all x1 -> x0, waiting for transfers between devices: 12.2 us -> none  [sum_at_owner(): blocks = lax.all_to_all(in_blocks(array, dim, size), axis, 0, 0, tiled=True)]
    ppermute x1 -> x0, starting transfers between devices: 3.79 us -> none  [from_behind(): return lax.ppermute(block, axis, route)]
    ppermute x1 -> x0, waiting for transfers between devices: 3.01 us -> none  [from_behind(): return lax.ppermute(block, axis, route)]
    unnamed x21 -> x16, local copies, waits for them, and re-layouts: 4.31 us -> 7.06 us
    dot_general x2 -> x0, matrix products: 1.94 us -> none  [the longest x1 1.51 us: local(): jnp.dot(resid_grad, mixed, preferred_element_type=jnp.float32)]
  transfers between devices with their start and end apart: 2 -> 0, of which waited for: 2 -> 0; matrix products, arithmetic and copies ran while one was open for 1% -> 0% of each run, Pallas kernels for 0% -> 0%
where the time goes in v2:
time: 120 us
  Pallas kernels  112 us (93%)
  local copies, waits for them, and re-layouts  7.06 us (6%)
    pallas_call x1, Pallas kernels, local(): pl.pallas_call(backward_kernel, out_shape=(grad, grad, grad, jax.ShapeDty...  112 us
    unnamed x16, local copies, waits for them, and re-layouts  7.06 us

profile of v2, /device:TPU:1, one launch (start us, length us, event | category | flops | bytes accessed | tf_op | source)
XLA Modules:
  0.0 119.6 jit_solution(11259389781945965689)
XLA Ops:
  0.6 111.9 %backward.1 = (bf16[224,2048]{1,0:T(8,128)(2,1)}, bf16[224,2048]{1,0:T(8,128)(2,1)}, bf16[224,2048]{1,0:T(8,128)(2,1)}, f32[32,256]{1,0:T(8,128)}, bf16[128,256]{1,0:T(8,128)(2,1)}, /*index=5*/bf16[128,256]{1,0:T(8,128)(2,1)}) custom-call(s32[2,128]{1,0:T(2,128)} %bitcast.23, f32[2,128]{1,0:T(2,128)} %bitcast.24, bf16[128,256]{1,0:T(8,128)(2,1)} %conv_ref.1, ...), custom_call_target="tpu_custom_call" | custom-call | tf_op jit(solution)/shard_map/backward/pallas_call | solution.py:615
  112.5 0.0 copy-start.1
  112.5 2.3 %copy.25 = bf16[1,2048,224]{1,2,0:T(8,128)(2,1)} copy(bf16[1,2048,224]{1,2,0:T(8,128)(2,1)} %bitcast.22) | data formatting | bytes 1835008
  114.8 0.0 copy-done.1
  114.8 0.0 copy-start
  114.8 0.9 copy.26
  115.7 0.6 copy-done
  116.3 0.0 copy-start.4
  116.3 0.9 copy.27
  117.2 0.0 copy-done.4
  117.3 0.0 copy-start.3
  117.3 0.6 copy.28
  117.9 0.2 copy-done.3
  118.1 0.0 copy-start.2
  118.1 0.6 copy.29
  118.7 0.2 copy-done.2
  119.0 0.6 copy.30
Async XLA Ops:
  112.5 2.3 %copy-start.1 = (bf16[224,2048]{1,0:T(8,128)(2,1)S(1)}, bf16[224,2048]{1,0:T(8,128)(2,1)}, u32[]{:S(2)}) copy-start(bf16[224,2048]{1,0:T(8,128)(2,1)} %get-tuple-element.13) | copy-start | bytes 2752516
  114.8 1.5 %copy-start = (bf16[224,2048]{1,0:T(8,128)(2,1)S(1)}, bf16[224,2048]{1,0:T(8,128)(2,1)}, u32[]{:S(2)}) copy-start(bf16[224,2048]{1,0:T(8,128)(2,1)} %get-tuple-element.14) | copy-start | bytes 2752516
  116.3 0.9 copy-start.4
  117.3 0.9 copy-start.3
  118.1 0.9 copy-start.2

commit v3 on v2

--- a/solution.py
+++ b/solution.py
@@ -24,14 +24,14 @@
 
 
 def backward_kernel(
-    routes_ref, weight_ref, conv_ref, value_ref, gate_ref, taps_ref, gain_ref,
-    x_hbm, cot_hbm, wg_hbm, wu_hbm, wd_hbm, proj_hbm,
-    gg_hbm, gu_hbm, gd_hbm, gp_ref, gv_ref, gt_ref,
-    xq, cq, perm, sendbuf, xc, wg, wu, wd, act_t, dg_t, du_t, gout,
+    routes_ref, weight_ref, gain_ref,
+    x_hbm, cot_hbm, wg_hbm, wu_hbm, wd_hbm, proj_hbm, conv_hbm, value_hbm, gate_hbm, taps_hbm,
+    gg_ref, gu_ref, gd_ref, gp_ref, gv_ref, gt_ref,
+    xq, cq, perm, sendbuf, xc, wg, wu, wd, act_t, dg_t, du_t,
     part, sib_in, in_a, in_b, in_c, in_d, in_e, total, ret,
-    res_ref, proj, normed, slope, mixed, scale, st_out, st_in, ext, halo_out, halo_in,
+    conv_ref, value_ref, gate_ref, taps_ref, res_ref, proj, normed, slope, mixed, scale, st_out, st_in, ext, halo_out, halo_in,
     gp, gp_sib, gp_x, gp_row, gp_z,
-    load_sem, out_sem, own_sem, a2a_send, a2a_recv, ag_send, ag_recv,
+    load_sem, own_sem, a2a_send, a2a_recv, ag_send, ag_recv,
     sb_send, sb_recv, rs_send, rs_recv, ret_send, ret_recv, res_send, res_recv,
     st_send, st_recv, halo_sem, gs_send, gs_recv, gx_send, gx_recv, gz_send, gz_recv,
 ):
@@ -99,8 +99,16 @@
     ]
     for copy in loads:
         copy.start()
-    load_proj = pltpu.make_async_copy(proj_hbm, proj, load_sem.at[5])
-    load_proj.start()
+    load_conv = pltpu.make_async_copy(conv_hbm, conv_ref, load_sem.at[5])
+    load_conv.start()
+    late_loads = [
+        pltpu.make_async_copy(src, dst, load_sem.at[6 + i])
+        for i, (src, dst) in enumerate((
+            (proj_hbm, proj), (value_hbm, value_ref), (gate_hbm, gate_ref), (taps_hbm, taps_ref)
+        ))
+    ]
+    for copy in late_loads:
+        copy.start()
 
     r0 = routes_ref[0:1, :]
     r1 = routes_ref[1:2, :]
@@ -187,6 +195,7 @@
         tall = jnp.concatenate([tot, jnp.zeros((120, 128), F32)], axis=0).T
         return tall[:, 0:1], tall[:, 1:2]
 
+    load_conv.wait()
     conv_vals = conv_ref[...].astype(F32)
     stats = sums_out(
         0,
@@ -366,24 +375,18 @@
     pair_sum(og, 3)
     pair_sum(g, 3)
 
-    def weight_grad(i, source, a):
+    def weight_grad(out_ref, source, a):
         def tile(q, _):
             acc = mm(source[0], xc[a, 0, q], NN)
             for m in range(1, 4):
                 acc += mm(source[m], xc[a, m, q], NN)
-            gout[i, :, pl.ds(pl.multiple_of(q * 512, 512), 512)] = acc.astype(BF)
+            out_ref[:, pl.ds(pl.multiple_of(q * 512, 512), 512)] = acc.astype(BF)
             return 0
 
         lax.fori_loop(0, 4, tile, 0)
 
-    weight_grad(0, dg_t, 0)
-    outs = [
-        pltpu.make_async_copy(gout.at[i], ref, out_sem.at[i])
-        for i, ref in enumerate((gg_hbm, gu_hbm, gd_hbm))
-    ]
-    outs[0].start()
-    weight_grad(1, du_t, 0)
-    outs[1].start()
+    weight_grad(gg_ref, dg_t, 0)
+    weight_grad(gu_ref, du_t, 0)
     send_a.wait_recv()
     part[m_g, y2] = (part[m_g, y2].astype(F32) + in_a[...].astype(F32)).astype(BF)
     send_cp = rs_copy(3, part.at[m_g, y2, first], in_c.at[0], dev_p)
@@ -397,8 +400,7 @@
     ).astype(BF)
     send_d = rs_copy(5, part.at[m_o, y], in_d, dev_x)
     send_d.start()
-    weight_grad(2, act_t, 1)
-    outs[2].start()
+    weight_grad(gd_ref, act_t, 1)
     send_cp.wait_recv()
     part[m_g, yp, first] = (part[m_g, yp, first].astype(F32) + in_c[0].astype(F32)).astype(BF)
     send_ep = rs_copy(6, part.at[m_g, yp], in_e.at[0], dev_p)
@@ -443,15 +445,33 @@
     def res_copy(kind, ref, dev):
         return remote(ref, ref, res_send.at[kind], res_recv.at[kind], dev)
 
-    sends = [res_copy(0, res_ref.at[y], dev_p), res_copy(1, res_ref.at[y], dev_m)]
-    sends[0].start()
-    sends[1].start()
-    load_proj.wait()
+    def res_out(kind):
+        ref, dev = (
+            (res_ref.at[y, half0], dev_p), (res_ref.at[y, half1], dev_p),
+            (res_ref.at[y, half1], dev_m), (res_ref.at[y, half0], dev_m),
+            (res_ref.at[ym, half0], dev_p), (res_ref.at[yp, half1], dev_m),
+        )[kind]
+        return res_copy(kind, ref, dev)
+
+    def res_in(kind):
+        ref, dev = (
+            (res_ref.at[ym, half0], dev_m), (res_ref.at[ym, half1], dev_m),
+            (res_ref.at[yp, half1], dev_p), (res_ref.at[yp, half0], dev_p),
+            (res_ref.at[y2, half0], dev_m), (res_ref.at[y2, half1], dev_p),
+        )[kind]
+        return res_copy(kind, ref, dev)
+
+    for kind in (0, 2, 1, 3):
+        res_out(kind).start()
+    for copy in late_loads:
+        copy.wait()
+
+    def pair_of(q):
+        return pl.ds(q * 2, 2)
 
     def gp_copy(q, j):
-        pair = pl.ds(q * 2, 2)
         return remote(
-            gp.at[oc, :, pair], gp_sib.at[:, pair], gs_send.at[j], gs_recv.at[j], dev_s
+            gp.at[oc, :, pair_of(q)], gp_sib.at[:, pair_of(q)], gs_send.at[j], gs_recv.at[j], dev_s
         )
 
     def proj_terms(q, j):
@@ -463,17 +483,51 @@
         gp_copy(q, j).start()
         return mm(feats, proj[pl.ds(pl.multiple_of(q * 512, 512), 512), :], NN)
 
+    def gx_copy(q, j, i):
+        return remote(
+            gp.at[c, others_x[i], pair_of(q)], gp_x.at[i, pair_of(q)],
+            gx_send.at[j, i], gx_recv.at[j, i], at_x(others_x[i]),
+        )
+
+    def over_x(q, j):
+        gp_copy(q, j).wait_recv()
+        gp[c, :, pair_of(q)] = (
+            gp[c, :, pair_of(q)].astype(F32) + gp_sib[:, pair_of(q)].astype(F32)
+        ).astype(BF)
+        for i in (1, 2, 0):
+            gx_copy(q, j, i).start()
+
+    def gz_copy(to, slot):
+        return remote(gp_row.at[to], gp_z.at[slot], gz_send.at[to], gz_recv.at[slot], at_z(to))
+
+    def over_z(q, j):
+        for i in range(3):
+            gx_copy(q, j, i).wait_recv()
+        pair = pair_of(q)
+        gp_row[pair] = (
+            (gp[c, x, pair].astype(F32) + gp_x[0, pair].astype(F32))
+            + (gp_x[1, pair].astype(F32) + gp_x[2, pair].astype(F32))
+        ).astype(BF)
+        for i in range(2):
+
+            @pl.when(q * 2 + i != z)
+            def _():
+                gz_copy(q * 2 + i, z).start()
+
     d_mixed = proj_terms(y, 0)
-    res_copy(0, res_ref.at[ym], dev_m).wait_recv()
-    sends.append(res_copy(2, res_ref.at[ym, half0], dev_p))
-    sends[2].start()
-    res_copy(1, res_ref.at[yp], dev_p).wait_recv()
-    sends.append(res_copy(3, res_ref.at[yp, half1], dev_m))
-    sends[3].start()
+    res_in(0).wait_recv()
+    res_out(4).start()
+    res_in(2).wait_recv()
+    res_out(5).start()
+    over_x(y, 0)
+    res_in(1).wait_recv()
     d_mixed += proj_terms(ym, 1)
+    res_in(3).wait_recv()
     d_mixed += proj_terms(yp, 2)
-    res_copy(2, res_ref.at[y2, half0], dev_m).wait_recv()
-    res_copy(3, res_ref.at[y2, half1], dev_p).wait_recv()
+    over_x(ym, 1)
+    over_x(yp, 2)
+    res_in(4).wait_recv()
+    res_in(5).wait_recv()
     d_mixed += proj_terms(y2, 3)
     d_norm = d_mixed * slope[...]
     norm_val = normed[...]
@@ -484,22 +538,10 @@
     )
     for copy in stats2:
         copy.start()
-
-    for j, q in enumerate((y, ym, yp, y2)):
-        gp_copy(q, j).wait_recv()
-
-    def pair_rows(xx):
-        gp[c, xx] = (gp[c, xx].astype(F32) + gp_sib[xx].astype(F32)).astype(BF)
-
-    def gx_copy(j):
-        return remote(
-            gp.at[c, others_x[j]], gp_x.at[j], gx_send.at[j], gx_recv.at[j], at_x(others_x[j])
-        )
-
-    for j in (1, 2, 0):
-        pair_rows(others_x[j])
-        gx_copy(j).start()
-    pair_rows(x)
+    over_x(y2, 3)
+    over_z(y, 0)
+    over_z(ym, 1)
+    over_z(yp, 2)
 
     first_sum, second_sum = sums_in(1, stats2)
     conv_grad = (
@@ -527,19 +569,7 @@
     glu_grads(0, 64, correlate(0, 64))
     glu_grads(64, 32, correlate(64, 32))
 
-    for j in range(3):
-        gx_copy(j).wait_recv()
-
-    def gz_copy(k):
-        zz = lax.rem(z + k, 8)
-        return remote(gp_row.at[zz], gp_z.at[k], gz_send.at[k], gz_recv.at[k], at_z(zz))
-
-    gp_row[...] = (
-        (gp[c, x].astype(F32) + gp_x[0].astype(F32)) + (gp_x[1].astype(F32) + gp_x[2].astype(F32))
-    ).astype(BF)
-    for k in (4, 3, 5, 2, 6, 1, 7):
-        gz_copy(k).start()
-
+    over_z(y2, 3)
     halo.wait_recv()
     keep = jnp.where(sp < 63, 1.0, 0.0)
     ext[128:160, :] = halo_in[...].astype(F32) * keep
@@ -547,12 +577,11 @@
 
     rows_sum = gp_row[z].astype(F32)
     for k in range(1, 8):
-        gz_copy(k).wait_recv()
-        rows_sum += gp_z[k].astype(F32)
+        zz = lax.rem(z + k, 8)
+        gz_copy(zz, zz).wait_recv()
+        rows_sum += gp_z[zz].astype(F32)
     gp_ref[...] = rows_sum
 
-    for copy in outs:
-        copy.wait()
     for a in range(2):
 
         def drain(k, _, a=a):
@@ -578,16 +607,26 @@
     for gg in (g, og):
         for j, yy in enumerate(order):
             sib_copy(gg, j, yy).wait_send()
-    for copy in (send_a, send_bp, send_bm, send_cp, send_cm, send_d, send_ep, send_em, *sends):
+    for copy in (send_a, send_bp, send_bm, send_cp, send_cm, send_d, send_ep, send_em):
         copy.wait_send()
     for copy in (*stats, *stats2, halo):
         copy.wait_send()
+    for kind in range(6):
+        res_out(kind).wait_send()
     for j, q in enumerate((y, ym, yp, y2)):
         gp_copy(q, j).wait_send()
-    for j in range(3):
-        gx_copy(j).wait_send()
+        for i in range(3):
+            gx_copy(q, j, i).wait_send()
     for k in range(1, 8):
-        gz_copy(k).wait_send()
+        gz_copy(lax.rem(z + k, 8), z).wait_send()
+
+
+def write_kernel(*refs):
+    copies = [pltpu.make_async_copy(refs[i], refs[6 + i], refs[12].at[i]) for i in range(6)]
+    for copy in copies:
+        copy.start()
+    for copy in copies:
+        copy.wait()
 
 
 def local(
@@ -612,11 +651,12 @@
     dma = pltpu.SemaphoreType.DMA
     grad = jax.ShapeDtypeStruct((units, width), BF)
     glu = jax.ShapeDtypeStruct((tokens, channels), BF)
-    gg, gu, gd, gp, gv, gt = pl.pallas_call(
+    shapes = (grad, grad, grad, jax.ShapeDtypeStruct((32, channels), F32), glu, glu)
+    results = pl.pallas_call(
         backward_kernel,
-        out_shape=(grad, grad, grad, jax.ShapeDtypeStruct((32, channels), F32), glu, glu),
-        in_specs=[vmem] * 7 + [hbm] * 6,
-        out_specs=(hbm, hbm, hbm, vmem, vmem, vmem),
+        out_shape=[pltpu.VMEM(a.shape, a.dtype) for a in shapes],
+        in_specs=[vmem] * 3 + [hbm] * 10,
+        out_specs=[vmem] * 6,
         scratch_shapes=[
             pltpu.VMEM((128, 512), BF),
             pltpu.VMEM((128, 512), BF),
@@ -629,7 +669,6 @@
             pltpu.VMEM((4, units, 256), BF),
             pltpu.VMEM((4, units, 256), BF),
             pltpu.VMEM((4, units, 256), BF),
-            pltpu.VMEM((3, units, width), BF),
             pltpu.VMEM((4, 4, 256, 512), BF),
             pltpu.VMEM((2, 4, 256, 512), BF),
             pltpu.VMEM((256, 512), BF),
@@ -639,6 +678,10 @@
             pltpu.VMEM((2, 256, 512), BF),
             pltpu.VMEM((256, 512), BF),
             pltpu.VMEM((256, 512), BF),
+            pltpu.VMEM((tokens, channels), BF),
+            pltpu.VMEM((tokens, channels), BF),
+            pltpu.VMEM((tokens, channels), BF),
+            pltpu.VMEM((WIDTH, channels), F32),
             pltpu.VMEM((4, 128, 512), BF),
             pltpu.VMEM((width, 256), BF),
             pltpu.VMEM((128, 256), F32),
@@ -655,21 +698,31 @@
             pltpu.VMEM((3, 8, 32, 256), BF),
             pltpu.VMEM((8, 32, 256), BF),
             pltpu.VMEM((8, 32, 256), BF),
-            dma((6,)), dma((3,)), dma((2,)),
+            dma((10,)), dma((2,)),
             dma((2, 16)), dma((2, 16)), dma((2, 16)), dma((2, 16)),
             dma((2, 4)), dma((2, 4)), dma((8,)), dma((8,)),
-            dma((16,)), dma((16,)), dma((4,)), dma((4,)),
+            dma((16,)), dma((16,)), dma((6,)), dma((6,)),
             dma((2, 3)), dma((2, 3)), dma((2,)),
-            dma((4,)), dma((4,)), dma((3,)), dma((3,)), dma((8,)), dma((8,)),
+            dma((4,)), dma((4,)), dma((4, 3)), dma((4, 3)), dma((8,)), dma((8,)),
         ],
         compiler_params=pltpu.CompilerParams(
             collective_id=0, has_side_effects=True, vmem_limit_bytes=60 * 1024 * 1024
         ),
         name="backward",
     )(
-        routes.T, route_weight.T, conv_out, glu_value, glu_gate, taps, norm_gain[None, :],
+        routes.T, route_weight.T, norm_gain[None, :],
         moe_input, out_cotangent, w_gate[0].T, w_up[0].T, w_down[0], out_proj,
+        conv_out, glu_value, glu_gate, taps,
     )
+    gg, gu, gd, gp, gv, gt = pl.pallas_call(
+        write_kernel,
+        out_shape=shapes,
+        in_specs=[vmem] * 6,
+        out_specs=[hbm] * 6,
+        scratch_shapes=[dma((6,))],
+        compiler_params=pltpu.CompilerParams(vmem_limit_bytes=1024 * 1024),
+        name="write_out",
+    )(*(pltpu.with_memory_space_constraint(r, pltpu.VMEM) for r in results))
     return (gg.T[None], gu.T[None], gd[None], gp, gv, gt)
 
 

time: 120 us -> 106 us (0.88)
  the two profiles are of different devices: /device:TPU:1 before, /device:TPU:16 now
where the time goes in v3:
time: 106 us; the launch traced here: 105 us
  Pallas kernels  105 us (99%)
    pallas_call x1, Pallas kernels, local(): pl.pallas_call(backward_kernel, out_shape=[pltpu.VMEM(a.shape, a.dtype) f...  103 us

profile of v3, /device:TPU:16, one launch (start us, length us, event | category | flops | bytes accessed | tf_op | source)
XLA Modules:
  0.0 105.4 jit_solution(17252730864106292345)
XLA Ops:
  0.6 103.1 %backward.1 = (bf16[224,2048]{1,0:T(8,128)(2,1)S(1)}, bf16[224,2048]{1,0:T(8,128)(2,1)S(1)}, bf16[224,2048]{1,0:T(8,128)(2,1)S(1)}, f32[32,256]{1,0:T(8,128)S(1)...) custom-call(s32[2,128]{1,0:T(2,128)} %bitcast.20, f32[2,128]{1,0:T(2,128)} %bitcast.21, f32[1,256]{1,0:T(1,128)} %bitcast.22, ...), custom_call_target="tpu_custom_call" | custom-call | tf_op jit(solution)/shard_map/backward/pallas_call | solution.py:655
  103.8 1.6 %write_out.1 = (bf16[224,2048]{1,0:T(8,128)(2,1)}, bf16[224,2048]{1,0:T(8,128)(2,1)}, bf16[224,2048]{1,0:T(8,128)(2,1)}, f32[32,256]{1,0:T(8,128)}, bf16[128,256]{1,0:T(8,128)(2,1)}, /*index=5*/bf16[128,256]{1,0:T(8,128)(2,1)}) custom-call(bf16[224,2048]{1,0:T(8,128)(2,1)S(1)} %get-tuple-element.18.refs_0_, bf16[224,2048]{1,0:T(8,128)(2,1)S(1)} %get-tuple-element.19.refs_1_, ...), custom_call_target="tpu_custom_call" | custom-call | tf_op jit(solution)/shard_map/write_out/pallas_call | solution.py:717

commit v4 on v3

--- a/solution.py
+++ b/solution.py
@@ -10,6 +10,7 @@
 MESH = pl.DeviceIdType.MESH
 BF = jnp.bfloat16
 F32 = jnp.float32
+NEAR = (0, 1, 7, 2, 6, 3, 5, 4)
 NT = (((1,), (1,)), ((), ()))
 NN = (((1,), (0,)), ((), ()))
 TN = (((0,), (0,)), ((), ()))
@@ -48,10 +49,14 @@
     me = sp // 4
     yp, ym, y2 = lax.rem(y + 1, 4), lax.rem(y + 3, 4), lax.rem(y + 2, 4)
 
-    def holder(q):
-        qh = lax.rem(q, 2)
-        qx = qh * 2 + lax.rem(g + qh, 2)
-        return ((q // 2) * 8 + qx * 2 + c, y)
+    def holder(zz, hh):
+        return (zz * 8 + (hh * 2 + lax.rem(g + hh, 2)) * 2 + c, y)
+
+    def to_of(p):
+        return lax.rem(z + 8 - NEAR[p // 2], 8), (xh if p % 2 == 0 else 1 - xh)
+
+    def from_of(p):
+        return lax.rem(z + NEAR[p // 2], 8), (xh if p % 2 == 0 else 1 - xh)
 
     dev_x = (z * 8 + (xh * 2 + 1 - xl) * 2 + c, y)
     dev_s = (z * 8 + x * 2 + oc, y)
@@ -76,11 +81,8 @@
 
     barrier = pltpu.get_barrier_semaphore()
 
-    def greet(k, _):
-        pl.semaphore_signal(barrier, inc=1, device_id=holder(lax.rem(me + k, 16)), device_id_type=MESH)
-        return 0
-
-    lax.fori_loop(1, 16, greet, 0)
+    for p in range(1, 16):
+        pl.semaphore_signal(barrier, inc=1, device_id=holder(*to_of(p)), device_id_type=MESH)
     greeted = (
         dev_x, dev_s, dev_p, dev_m, dev_2, at_x(others_x[1]), at_x(others_x[2]), dev_prev, dev_next
     )
@@ -144,37 +146,33 @@
     def rows_of(q):
         return pl.ds(pl.multiple_of(q * 16, 16), 16)
 
-    for a in range(2):
-
-        def push(k, _, a=a):
-            q = lax.rem(me + k, 16)
-            remote(
-                sendbuf.at[a, rows_of(q)], xc.at[a, m_own, y, rows_of(me)],
-                a2a_send.at[a, q], a2a_recv.at[a, me], holder(q),
-            ).start()
-            return 0
-
-        lax.fori_loop(1, 16, push, 0)
+    def place_of(a, p):
+        return xc.at[a, p // 8, m_own, y, pl.ds(p % 8 * 16, 16)]
+
+    def out_copy(a, p):
+        zz, hh = to_of(p)
+        return remote(
+            sendbuf.at[a, rows_of(zz * 2 + hh)], place_of(a, p),
+            a2a_send.at[a, p], a2a_recv.at[a, p], holder(zz, hh),
+        )
+
+    def a2a_wait(a, h):
+        for p in range(8 * h, 8 * h + 8):
+            if p == 0:
+                own[a].wait()
+            else:
+                out_copy(a, p).wait_recv()
+
     own = [
-        pltpu.make_async_copy(
-            sendbuf.at[a, rows_of(me)], xc.at[a, m_own, y, rows_of(me)], own_sem.at[a]
-        )
+        pltpu.make_async_copy(sendbuf.at[a, rows_of(me)], place_of(a, 0), own_sem.at[a])
         for a in range(2)
     ]
-    own[0].start()
-    own[1].start()
-
-    def a2a_wait(a):
-        def one(k, _):
-            q = lax.rem(me + 16 - k, 16)
-            remote(
-                sendbuf.at[a, rows_of(q)], xc.at[a, m_own, y, rows_of(q)],
-                a2a_send.at[a, q], a2a_recv.at[a, q], holder(q),
-            ).wait_recv()
-            return 0
-
-        lax.fori_loop(1, 16, one, 0)
-        own[a].wait()
+    for h in range(2):
+        for a in range(2):
+            if h == 0:
+                own[a].start()
+            for p in range(max(8 * h, 1), 8 * h + 8):
+                out_copy(a, p).start()
 
     lane = lax.broadcasted_iota(jnp.int32, (128, 128), 1)
 
@@ -205,71 +203,235 @@
     for copy in stats:
         copy.start()
 
-    first, second = pl.ds(0, 128), pl.ds(128, 128)
+    first, second = pl.ds(0, 64), pl.ds(64, 64)
     listed = [(g, y), (g, ym), (g, yp), (g, y2), (og, y), (og, ym), (og, yp), (og, y2)]
 
-    def block(a, gg, cc, yy):
-        return xc.at[a, gg * 2 + cc, yy]
-
-    def ag_copy(a, kind, ref, dev):
-        return remote(ref, ref, ag_send.at[a, kind], ag_recv.at[a, kind], dev)
-
-    def ag_out(a, kind):
+    def block(a, h, gg, cc, yy):
+        return xc.at[a, h, gg * 2 + cc, yy]
+
+    def ag_copy(a, h, kind, ref, dev):
+        return remote(ref, ref, ag_send.at[a * 2 + h, kind], ag_recv.at[a * 2 + h, kind], dev)
+
+    def ag_out(a, h, kind):
         if kind >= 8:
             gg, yy = listed[kind - 8]
-            return ag_copy(a, kind, block(a, gg, c, yy), dev_s)
+            return ag_copy(a, h, kind, block(a, h, gg, c, yy), dev_s)
         ref, dev = (
-            (block(a, g, c, y), dev_x),
-            (block(a, g, c, y), dev_p),
-            (block(a, g, c, y), dev_m),
-            (block(a, g, c, ym).at[first], dev_p),
-            (block(a, g, c, yp).at[second], dev_m),
-            (block(a, og, c, y), dev_p),
-            (block(a, og, c, y), dev_m),
-            (block(a, g, c, y2), dev_x),
+            (block(a, h, g, c, y), dev_x),
+            (block(a, h, g, c, y), dev_p),
+            (block(a, h, g, c, y), dev_m),
+            (block(a, h, g, c, ym).at[first], dev_p),
+            (block(a, h, g, c, yp).at[second], dev_m),
+            (block(a, h, og, c, y), dev_p),
+            (block(a, h, og, c, y), dev_m),
+            (block(a, h, g, c, y2), dev_x),
         )[kind]
-        return ag_copy(a, kind, ref, dev)
-
-    def ag_in(a, kind):
+        return ag_copy(a, h, kind, ref, dev)
+
+    def ag_in(a, h, kind):
         if kind >= 8:
             gg, yy = listed[kind - 8]
-            return ag_copy(a, kind, block(a, gg, oc, yy), dev_s)
+            return ag_copy(a, h, kind, block(a, h, gg, oc, yy), dev_s)
         ref, dev = (
-            (block(a, og, c, y), dev_x),
-            (block(a, g, c, ym), dev_m),
-            (block(a, g, c, yp), dev_p),
-            (block(a, g, c, y2).at[first], dev_m),
-            (block(a, g, c, y2).at[second], dev_p),
-            (block(a, og, c, ym), dev_m),
-            (block(a, og, c, yp), dev_p),
-            (block(a, og, c, y2), dev_x),
+            (block(a, h, og, c, y), dev_x),
+            (block(a, h, g, c, ym), dev_m),
+            (block(a, h, g, c, yp), dev_p),
+            (block(a, h, g, c, y2).at[first], dev_m),
+            (block(a, h, g, c, y2).at[second], dev_p),
+            (block(a, h, og, c, ym), dev_m),
+            (block(a, h, og, c, yp), dev_p),
+            (block(a, h, og, c, y2), dev_x),
         )[kind]
-        return ag_copy(a, kind, ref, dev)
-
-    def go(a, *kinds):
+        return ag_copy(a, h, kind, ref, dev)
+
+    def go(a, h, *kinds):
         for kind in kinds:
-            ag_out(a, kind).start()
-
-    def got(a, *kinds):
+            ag_out(a, h, kind).start()
+
+    def got(a, h, *kinds):
         for kind in kinds:
-            ag_in(a, kind).wait_recv()
-
-    a2a_wait(0)
-    go(0, 0, 1, 2, 8)
-    a2a_wait(1)
-    go(1, 0, 1, 2, 8)
-    got(0, 1)
-    go(0, 3, 9)
-    got(0, 2)
-    go(0, 4, 10)
-    got(1, 1)
-    go(1, 3, 9)
-    got(1, 2)
-    go(1, 4, 10)
-    got(0, 0)
-    go(0, 5, 6, 12)
-    got(1, 0)
-    go(1, 5, 6, 12)
+            ag_in(a, h, kind).wait_recv()
+
+    def relay_y(a, h):
+        got(a, h, 1)
+        go(a, h, 3, 9)
+        got(a, h, 2)
+        go(a, h, 4, 10)
+
+    def relay_x(a, h):
+        got(a, h, 0)
+        go(a, h, 5, 6, 12)
+
+    def relay_far(a, h):
+        got(a, h, 3, 4)
+        go(a, h, 7, 11)
+
+    def relay_last(a, h):
+        got(a, h, 5)
+        go(a, h, 13)
+        got(a, h, 6)
+        go(a, h, 14)
+        got(a, h, 7)
+        go(a, h, 15)
+
+    def pair(gg):
+        return pl.ds(gg * 2, 2)
+
+    def rows_at(a, h, gg, q):
+        return xc[a, h, pair(gg), q].reshape(256, 512)
+
+    def forward(h, gg):
+        pre_g = jnp.zeros((256, 224), F32)
+        pre_u = jnp.zeros((256, 224), F32)
+        d_act = jnp.zeros((256, 224), F32)
+        for q in range(4):
+            span = slice(q * 512, q * 512 + 512)
+            rows = rows_at(0, h, gg, q)
+            pre_g += mm(rows, wg[:, span], NT)
+            pre_u += mm(rows, wu[:, span], NT)
+            d_act += mm(rows_at(1, h, gg, q), wd[:, span], NT)
+        sig = jax.nn.sigmoid(pre_g)
+        d_gate = (d_act * pre_u * swish_slope(pre_g, sig)).astype(BF)
+        d_up = (d_act * pre_g * sig).astype(BF)
+        slot = h * 2 + gg
+        act_t[slot] = (pre_g * sig * pre_u).T.astype(BF)
+        dg_t[slot] = d_gate.T
+        du_t[slot] = d_up.T
+        return d_gate, d_up
+
+    def back(h, gg, grads, yy):
+        span = pl.ds(pl.multiple_of(yy * 512, 512), 512)
+        term = mm(grads[0], wg[:, span], NN) + mm(grads[1], wu[:, span], NN)
+        part[h, pair(gg), yy] = term.astype(BF).reshape(2, 128, 512)
+
+    order = (y2, yp, ym, y)
+
+    def sib_copy(h, gg, j):
+        at = (0 if gg is g else 4) + j
+        return remote(
+            part.at[h, gg * 2 + oc, order[j]], sib_in.at[h, gg, order[j]],
+            sb_send.at[h, at], sb_recv.at[h, at], dev_s,
+        )
+
+    def whole(h, gg, *between):
+        grads = forward(h, gg)
+        for j in range(4):
+            back(h, gg, grads, order[j])
+            sib_copy(h, gg, j).start()
+            if j < len(between):
+                between[j]()
+
+    m_g, m_o = g * 2 + c, og * 2 + c
+
+    def pair_sum(h, gg, j):
+        sib_copy(h, gg, j).wait_recv()
+        at = (h, gg * 2 + c, order[j])
+        part[at] = (part[at].astype(F32) + sib_in[h, gg, order[j]].astype(F32)).astype(BF)
+
+    def rs_copy(h, kind):
+        src, dst, dev = (
+            (part.at[h, m_o, y2, first], in_a.at[h, first], dev_x),
+            (part.at[h, m_o, y2, second], in_a.at[h, second], dev_x),
+            (part.at[h, m_o, yp], in_b.at[h, 0], dev_p),
+            (part.at[h, m_o, ym], in_b.at[h, 1], dev_m),
+            (part.at[h, m_g, y2, first], in_c.at[h, 0], dev_p),
+            (part.at[h, m_g, y2, second], in_c.at[h, 1], dev_m),
+            (part.at[h, m_o, y], in_d.at[h], dev_x),
+            (part.at[h, m_g, yp, second], in_e.at[h, 0, second], dev_p),
+            (part.at[h, m_g, ym, first], in_e.at[h, 1, first], dev_m),
+            (part.at[h, m_g, yp, first], in_e.at[h, 0, first], dev_p),
+            (part.at[h, m_g, ym, second], in_e.at[h, 1, second], dev_m),
+        )[kind]
+        return remote(src, dst, rs_send.at[h, kind], rs_recv.at[h, kind], dev)
+
+    def rs_open(h):
+        pair_sum(h, og, 0)
+        rs_copy(h, 0).start()
+        rs_copy(h, 1).start()
+        pair_sum(h, og, 1)
+        rs_copy(h, 2).start()
+        pair_sum(h, og, 2)
+        rs_copy(h, 3).start()
+
+    def rs_own(h):
+        for j, kind in ((1, 7), (2, 8), (0, None)):
+            pair_sum(h, g, j)
+            if kind:
+                rs_copy(h, kind).start()
+        pair_sum(h, og, 3)
+        pair_sum(h, g, 3)
+
+    def add_to(at, *terms):
+        value = part[at].astype(F32)
+        for term in terms:
+            value += term.astype(F32)
+        part[at] = value.astype(BF)
+
+    def rs_far(h):
+        rs_copy(h, 0).wait_recv()
+        add_to((h, m_g, y2, first), in_a[h, first])
+        rs_copy(h, 4).start()
+        rs_copy(h, 1).wait_recv()
+        add_to((h, m_g, y2, second), in_a[h, second])
+        rs_copy(h, 5).start()
+
+    def rs_cross(h):
+        rs_copy(h, 2).wait_recv()
+        rs_copy(h, 3).wait_recv()
+        add_to((h, m_o, y), in_b[h, 0], in_b[h, 1])
+        rs_copy(h, 6).start()
+
+    def rs_near(h):
+        rs_copy(h, 4).wait_recv()
+        add_to((h, m_g, yp, first), in_c[h, 0])
+        rs_copy(h, 9).start()
+        rs_copy(h, 5).wait_recv()
+        add_to((h, m_g, ym, second), in_c[h, 1])
+        rs_copy(h, 10).start()
+
+    def ret_copy(p):
+        zz, hh = from_of(p)
+        return remote(
+            total.at[p // 8, pl.ds(p % 8 * 16, 16)], ret.at[rows_of(me)],
+            ret_send.at[p], ret_recv.at[p], holder(zz, hh),
+        )
+
+    own_back = pltpu.make_async_copy(total.at[0, pl.ds(0, 16)], ret.at[rows_of(me)], own_sem.at[0])
+
+    def rs_close(h):
+        for kind in range(6, 11):
+            rs_copy(h, kind).wait_recv()
+        total[h] = (
+            part[h, m_g, y].astype(F32) + in_d[h].astype(F32)
+            + in_e[h, 0].astype(F32) + in_e[h, 1].astype(F32)
+        ).astype(BF)
+        for p in range(8 * h, 8 * h + 8):
+            if p == 0:
+                own_back.start()
+            else:
+                ret_copy(p).start()
+
+    def weight_grad(out_ref, source, a):
+        def tile(q, _):
+            acc = jnp.zeros((source.shape[1], 512), F32)
+            for h in range(2):
+                for gg in range(2):
+                    acc += mm(source[h * 2 + gg], rows_at(a, h, gg, q), NN)
+            out_ref[:, pl.ds(pl.multiple_of(q * 512, 512), 512)] = acc.astype(BF)
+            return 0
+
+        lax.fori_loop(0, 4, tile, 0)
+
+    a2a_wait(0, 0)
+    go(0, 0, 0, 1, 2, 8)
+    a2a_wait(1, 0)
+    go(1, 0, 0, 1, 2, 8)
+    relay_y(0, 0)
+    relay_y(1, 0)
+    relay_x(0, 0)
+    relay_x(1, 0)
+    a2a_wait(0, 1)
+    go(0, 1, 0, 1, 2, 8)
     sum1, sum2 = sums_in(0, stats)
     mean = sum1 / DB
     rstd = lax.rsqrt(sum2 / DB - mean * mean + 1e-05)
@@ -280,162 +442,49 @@
     mixed[...] = (zpre * zsig).astype(BF)
     slope[...] = swish_slope(zpre, zsig) * gain_ref[...]
     scale[...] = jnp.broadcast_to(rstd, (128, 256))
-    got(0, 3, 4)
-    go(0, 7, 11)
-    got(1, 3, 4)
-    go(1, 7, 11)
-
+    relay_far(0, 0)
+    relay_far(1, 0)
+    a2a_wait(1, 1)
+    go(1, 1, 0, 1, 2, 8)
     for copy in loads:
         copy.wait()
-
-    def forward(m):
-        pre_g = jnp.zeros((256, 224), F32)
-        pre_u = jnp.zeros((256, 224), F32)
-        d_act = jnp.zeros((256, 224), F32)
-        for q in range(4):
-            span = slice(q * 512, q * 512 + 512)
-            rows = xc[0, m, q]
-            pre_g += mm(rows, wg[:, span], NT)
-            pre_u += mm(rows, wu[:, span], NT)
-            d_act += mm(xc[1, m, q], wd[:, span], NT)
-        sig = jax.nn.sigmoid(pre_g)
-        d_gate = (d_act * pre_u * swish_slope(pre_g, sig)).astype(BF)
-        d_up = (d_act * pre_g * sig).astype(BF)
-        act_t[m] = (pre_g * sig * pre_u).T.astype(BF)
-        dg_t[m] = d_gate.T
-        du_t[m] = d_up.T
-        return d_gate, d_up
-
-    def back(m, d_gate, d_up, yy):
-        span = pl.ds(pl.multiple_of(yy * 512, 512), 512)
-        part[m, yy] = (mm(d_gate, wg[:, span], NN) + mm(d_up, wu[:, span], NN)).astype(BF)
-
-    def sib_copy(gg, j, yy):
-        return remote(
-            part.at[gg * 2 + oc, yy], sib_in.at[gg, yy],
-            sb_send.at[gg, j], sb_recv.at[gg, j], dev_s,
-        )
-
-    order = (y2, yp, ym, y)
-
-    def whole(gg, cc, sent):
-        m = gg * 2 + cc
-        d_gate, d_up = forward(m)
-        for j, yy in enumerate(order):
-            back(m, d_gate, d_up, yy)
-            if sent:
-                sib_copy(gg, j, yy).start()
-
-    whole(g, c, False)
-    got(0, 8, 9, 10, 11)
-    got(1, 8, 9, 10, 11)
-    got(0, 5)
-    go(0, 13)
-    got(0, 6)
-    go(0, 14)
-    got(0, 7)
-    go(0, 15)
-    whole(g, oc, True)
-    got(1, 5)
-    go(1, 13)
-    got(1, 6)
-    go(1, 14)
-    got(1, 7)
-    go(1, 15)
-    whole(og, c, False)
-    got(0, 12, 13, 14, 15)
-    got(1, 12, 13, 14, 15)
-    whole(og, oc, True)
-
-    def pair_sum(gg, j):
-        yy = order[j]
-        sib_copy_in = remote(
-            part.at[gg * 2 + oc, yy], sib_in.at[gg, yy],
-            sb_send.at[gg, j], sb_recv.at[gg, j], dev_s,
-        )
-        sib_copy_in.wait_recv()
-        m = gg * 2 + c
-        part[m, yy] = (part[m, yy].astype(F32) + sib_in[gg, yy].astype(F32)).astype(BF)
-
-    def rs_copy(kind, src, dst, dev):
-        return remote(src, dst, rs_send.at[kind], rs_recv.at[kind], dev)
-
-    m_g, m_o = g * 2 + c, og * 2 + c
-    pair_sum(og, 0)
-    send_a = rs_copy(0, part.at[m_o, y2], in_a, dev_x)
-    send_a.start()
-    pair_sum(og, 1)
-    send_bp = rs_copy(1, part.at[m_o, yp], in_b.at[0], dev_p)
-    send_bp.start()
-    pair_sum(og, 2)
-    send_bm = rs_copy(2, part.at[m_o, ym], in_b.at[1], dev_m)
-    send_bm.start()
-    for j in range(3):
-        pair_sum(g, j)
-    pair_sum(og, 3)
-    pair_sum(g, 3)
-
-    def weight_grad(out_ref, source, a):
-        def tile(q, _):
-            acc = mm(source[0], xc[a, 0, q], NN)
-            for m in range(1, 4):
-                acc += mm(source[m], xc[a, m, q], NN)
-            out_ref[:, pl.ds(pl.multiple_of(q * 512, 512), 512)] = acc.astype(BF)
-            return 0
-
-        lax.fori_loop(0, 4, tile, 0)
-
+    got(0, 0, 8, 9, 10, 11)
+    got(1, 0, 8, 9, 10, 11)
+    whole(0, g)
+    relay_last(0, 0)
+    relay_last(1, 0)
+    relay_y(0, 1)
+    got(0, 0, 12, 13, 14, 15)
+    got(1, 0, 12, 13, 14, 15)
+    whole(0, og, lambda: relay_y(1, 1), lambda: relay_x(0, 1), lambda: relay_x(1, 1))
+    rs_open(0)
+    rs_own(0)
+    relay_far(0, 1)
+    relay_far(1, 1)
+    got(0, 1, 8, 9, 10, 11)
+    got(1, 1, 8, 9, 10, 11)
+    whole(1, g)
+    rs_far(0)
+    relay_last(0, 1)
+    relay_last(1, 1)
+    got(0, 1, 12, 13, 14, 15)
+    got(1, 1, 12, 13, 14, 15)
+    whole(1, og)
+    rs_open(1)
+    rs_cross(0)
+    rs_own(1)
+    rs_near(0)
     weight_grad(gg_ref, dg_t, 0)
     weight_grad(gu_ref, du_t, 0)
-    send_a.wait_recv()
-    part[m_g, y2] = (part[m_g, y2].astype(F32) + in_a[...].astype(F32)).astype(BF)
-    send_cp = rs_copy(3, part.at[m_g, y2, first], in_c.at[0], dev_p)
-    send_cm = rs_copy(4, part.at[m_g, y2, second], in_c.at[1], dev_m)
-    send_cp.start()
-    send_cm.start()
-    send_bp.wait_recv()
-    send_bm.wait_recv()
-    part[m_o, y] = (
-        part[m_o, y].astype(F32) + in_b[0].astype(F32) + in_b[1].astype(F32)
-    ).astype(BF)
-    send_d = rs_copy(5, part.at[m_o, y], in_d, dev_x)
-    send_d.start()
+    rs_far(1)
+    rs_cross(1)
+    rs_near(1)
+    rs_close(0)
     weight_grad(gd_ref, act_t, 1)
-    send_cp.wait_recv()
-    part[m_g, yp, first] = (part[m_g, yp, first].astype(F32) + in_c[0].astype(F32)).astype(BF)
-    send_ep = rs_copy(6, part.at[m_g, yp], in_e.at[0], dev_p)
-    send_ep.start()
-    send_cm.wait_recv()
-    part[m_g, ym, second] = (part[m_g, ym, second].astype(F32) + in_c[1].astype(F32)).astype(BF)
-    send_em = rs_copy(7, part.at[m_g, ym], in_e.at[1], dev_m)
-    send_em.start()
-    send_d.wait_recv()
-    send_ep.wait_recv()
-    send_em.wait_recv()
-    total[...] = (
-        part[m_g, y].astype(F32) + in_d[...].astype(F32)
-        + in_e[0].astype(F32) + in_e[1].astype(F32)
-    ).astype(BF)
-
-    def push_back(k, _):
-        q = lax.rem(me + k, 16)
-        remote(
-            total.at[rows_of(q)], ret.at[rows_of(me)], ret_send.at[q], ret_recv.at[me], holder(q)
-        ).start()
-        return 0
-
-    lax.fori_loop(1, 16, push_back, 0)
-    own_back = pltpu.make_async_copy(total.at[rows_of(me)], ret.at[rows_of(me)], own_sem.at[0])
-    own_back.start()
-
-    def wait_back(k, _):
-        q = lax.rem(me + 16 - k, 16)
-        remote(
-            total.at[rows_of(q)], ret.at[rows_of(q)], ret_send.at[q], ret_recv.at[q], holder(q)
-        ).wait_recv()
-        return 0
-
-    lax.fori_loop(1, 16, wait_back, 0)
+    rs_close(1)
+
+    for p in range(1, 16):
+        ret_copy(p).wait_recv()
     own_back.wait()
     moe = mm(perm[...], ret[...], TN)
     res_ref[y] = (cq[...].astype(F32) + moe).astype(BF)
@@ -583,32 +632,19 @@
     gp_ref[...] = rows_sum
 
     for a in range(2):
-
-        def drain(k, _, a=a):
-            q = lax.rem(me + k, 16)
-            remote(
-                sendbuf.at[a, rows_of(q)], xc.at[a, m_own, y, rows_of(me)],
-                a2a_send.at[a, q], a2a_recv.at[a, me], holder(q),
-            ).wait_send()
-            return 0
-
-        lax.fori_loop(1, 16, drain, 0)
-        for kind in range(16):
-            ag_out(a, kind).wait_send()
-
-    def drain_back(k, _):
-        q = lax.rem(me + k, 16)
-        remote(
-            total.at[rows_of(q)], ret.at[rows_of(me)], ret_send.at[q], ret_recv.at[me], holder(q)
-        ).wait_send()
-        return 0
-
-    lax.fori_loop(1, 16, drain_back, 0)
-    for gg in (g, og):
-        for j, yy in enumerate(order):
-            sib_copy(gg, j, yy).wait_send()
-    for copy in (send_a, send_bp, send_bm, send_cp, send_cm, send_d, send_ep, send_em):
-        copy.wait_send()
+        for p in range(1, 16):
+            out_copy(a, p).wait_send()
+        for h in range(2):
+            for kind in range(16):
+                ag_out(a, h, kind).wait_send()
+    for h in range(2):
+        for gg in (g, og):
+            for j in range(4):
+                sib_copy(h, gg, j).wait_send()
+        for kind in range(11):
+            rs_copy(h, kind).wait_send()
+    for p in range(1, 16):
+        ret_copy(p).wait_send()
     for copy in (*stats, *stats2, halo):
         copy.wait_send()
     for kind in range(6):
@@ -662,21 +698,21 @@
             pltpu.VMEM((128, 512), BF),
             pltpu.VMEM((256, 128), BF),
             pltpu.VMEM((2, 256, 512), BF),
-            pltpu.VMEM((2, 4, 4, 256, 512), BF),
+            pltpu.VMEM((2, 2, 4, 4, 128, 512), BF),
             pltpu.VMEM((units, width), BF),
             pltpu.VMEM((units, width), BF),
             pltpu.VMEM((units, width), BF),
             pltpu.VMEM((4, units, 256), BF),
             pltpu.VMEM((4, units, 256), BF),
             pltpu.VMEM((4, units, 256), BF),
-            pltpu.VMEM((4, 4, 256, 512), BF),
-            pltpu.VMEM((2, 4, 256, 512), BF),
-            pltpu.VMEM((256, 512), BF),
-            pltpu.VMEM((2, 256, 512), BF),
+            pltpu.VMEM((2, 4, 4, 128, 512), BF),
+            pltpu.VMEM((2, 2, 4, 128, 512), BF),
             pltpu.VMEM((2, 128, 512), BF),
-            pltpu.VMEM((256, 512), BF),
-            pltpu.VMEM((2, 256, 512), BF),
-            pltpu.VMEM((256, 512), BF),
+            pltpu.VMEM((2, 2, 128, 512), BF),
+            pltpu.VMEM((2, 2, 64, 512), BF),
+            pltpu.VMEM((2, 128, 512), BF),
+            pltpu.VMEM((2, 2, 128, 512), BF),
+            pltpu.VMEM((2, 128, 512), BF),
             pltpu.VMEM((256, 512), BF),
             pltpu.VMEM((tokens, channels), BF),
             pltpu.VMEM((tokens, channels), BF),
@@ -699,8 +735,8 @@
             pltpu.VMEM((8, 32, 256), BF),
             pltpu.VMEM((8, 32, 256), BF),
             dma((10,)), dma((2,)),
-            dma((2, 16)), dma((2, 16)), dma((2, 16)), dma((2, 16)),
-            dma((2, 4)), dma((2, 4)), dma((8,)), dma((8,)),
+            dma((2, 16)), dma((2, 16)), dma((4, 16)), dma((4, 16)),
+            dma((2, 8)), dma((2, 8)), dma((2, 11)), dma((2, 11)),
             dma((16,)), dma((16,)), dma((6,)), dma((6,)),
             dma((2, 3)), dma((2, 3)), dma((2,)),
             dma((4,)), dma((4,)), dma((4, 3)), dma((4, 3)), dma((8,)), dma((8,)),

time: 106 us -> 97.7 us (0.922)
  Pallas kernels: 105 us -> 96.8 us
    pallas_call x1, Pallas kernels: 103 us -> 95.2 us  [local(): pl.pallas_call(backward_kernel, out_shape=[pltpu.VMEM(a.shape, a.dtype) f...]
where the time goes in v4:
time: 97.7 us; the launch traced here: 97.6 us
  Pallas kernels  96.8 us (99%)
    pallas_call x1, Pallas kernels, local(): pl.pallas_call(backward_kernel, out_shape=[pltpu.VMEM(a.shape, a.dtype) f...  95.2 us

profile of v4, /device:TPU:16, one launch (start us, length us, event | category | flops | bytes accessed | tf_op | source)
XLA Modules:
  0.0 97.6 jit_solution(13730779154460103347)
XLA Ops:
  0.6 95.2 %backward.1 = (bf16[224,2048]{1,0:T(8,128)(2,1)S(1)}, bf16[224,2048]{1,0:T(8,128)(2,1)S(1)}, bf16[224,2048]{1,0:T(8,128)(2,1)S(1)}, f32[32,256]{1,0:T(8,128)S(1)...) custom-call(s32[2,128]{1,0:T(2,128)} %bitcast.20, f32[2,128]{1,0:T(2,128)} %bitcast.21, f32[1,256]{1,0:T(1,128)} %bitcast.22, ...), custom_call_target="tpu_custom_call" | custom-call | tf_op jit(solution)/shard_map/backward/pallas_call | solution.py:691
  95.8 1.6 %write_out.1 = (bf16[224,2048]{1,0:T(8,128)(2,1)}, bf16[224,2048]{1,0:T(8,128)(2,1)}, bf16[224,2048]{1,0:T(8,128)(2,1)}, f32[32,256]{1,0:T(8,128)}, bf16[128,256]{1,0:T(8,128)(2,1)}, /*index=5*/bf16[128,256]{1,0:T(8,128)(2,1)}) custom-call(bf16[224,2048]{1,0:T(8,128)(2,1)S(1)} %get-tuple-element.18.refs_0_, bf16[224,2048]{1,0:T(8,128)(2,1)S(1)} %get-tuple-element.19.refs_1_, ...), custom_call_target="tpu_custom_call" | custom-call | tf_op jit(solution)/shard_map/write_out/pallas_call | solution.py:753

commit v5 on v4

--- a/solution.py
+++ b/solution.py
@@ -25,14 +25,14 @@
 
 
 def backward_kernel(
-    routes_ref, weight_ref, gain_ref,
+    gain_ref, routes_hbm, weight_hbm,
     x_hbm, cot_hbm, wg_hbm, wu_hbm, wd_hbm, proj_hbm, conv_hbm, value_hbm, gate_hbm, taps_hbm,
     gg_ref, gu_ref, gd_ref, gp_ref, gv_ref, gt_ref,
-    xq, cq, perm, sendbuf, xc, wg, wu, wd, act_t, dg_t, du_t,
+    xq, cq, xq2, cq2, perm, sendbuf, sendbuf2, xc, wg, wu, wd, act_t, dg_t, du_t,
     part, sib_in, in_a, in_b, in_c, in_d, in_e, total, ret,
-    conv_ref, value_ref, gate_ref, taps_ref, res_ref, proj, normed, slope, mixed, scale, st_out, st_in, ext, halo_out, halo_in,
+    routes_ref, weight_ref, conv_ref, value_ref, gate_ref, taps_ref, res_ref, proj, normed, slope, mixed, scale, st_out, st_in, ext, halo_out, halo_in,
     gp, gp_sib, gp_x, gp_row, gp_z,
-    load_sem, own_sem, a2a_send, a2a_recv, ag_send, ag_recv,
+    load_sem, own_sem, a2a_send, a2a_recv, far_send, far_recv, ag_send, ag_recv,
     sb_send, sb_recv, rs_send, rs_recv, ret_send, ret_recv, res_send, res_recv,
     st_send, st_recv, halo_sem, gs_send, gs_recv, gx_send, gx_recv, gz_send, gz_recv,
 ):
@@ -79,21 +79,28 @@
             device_id_type=MESH,
         )
 
-    barrier = pltpu.get_barrier_semaphore()
-
-    for p in range(1, 16):
-        pl.semaphore_signal(barrier, inc=1, device_id=holder(*to_of(p)), device_id_type=MESH)
-    greeted = (
-        dev_x, dev_s, dev_p, dev_m, dev_2, at_x(others_x[1]), at_x(others_x[2]), dev_prev, dev_next
-    )
-    for dev in greeted:
-        pl.semaphore_signal(barrier, inc=1, device_id=dev, device_id_type=MESH)
-
+    def all_sent(ref, sem):
+        remote(ref, ref, sem, sem, dev_s).wait_send()
+
+    def all_in(ref, sem):
+        remote(ref, ref, sem, sem, dev_s).wait_recv()
+
+    load_r = pltpu.make_async_copy(routes_hbm, routes_ref, load_sem.at[12])
+    load_w = pltpu.make_async_copy(weight_hbm, weight_ref, load_sem.at[13])
+    load_r.start()
+    load_w.start()
     cols = pl.ds(pl.multiple_of(y * 512, 512), 512)
     load_x = pltpu.make_async_copy(x_hbm.at[:, cols], xq, load_sem.at[0])
     load_c = pltpu.make_async_copy(cot_hbm.at[:, cols], cq, load_sem.at[1])
     load_x.start()
     load_c.start()
+    cols2 = pl.ds(pl.multiple_of(y2 * 512, 512), 512)
+    load_far = [
+        pltpu.make_async_copy(x_hbm.at[:, cols2], xq2, load_sem.at[10]),
+        pltpu.make_async_copy(cot_hbm.at[:, cols2], cq2, load_sem.at[11]),
+    ]
+    for copy in load_far:
+        copy.start()
     loads = [
         pltpu.make_async_copy(wg_hbm, wg, load_sem.at[2]),
         pltpu.make_async_copy(wu_hbm, wu, load_sem.at[3]),
@@ -111,6 +118,19 @@
     ]
     for copy in late_loads:
         copy.start()
+
+    barrier = pltpu.get_barrier_semaphore()
+
+    for p in range(1, 16):
+        pl.semaphore_signal(barrier, inc=1, device_id=holder(*to_of(p)), device_id_type=MESH)
+    greeted = (
+        dev_x, dev_s, dev_p, dev_m, dev_2, at_x(others_x[1]), at_x(others_x[2]), dev_prev, dev_next
+    )
+    for dev in greeted:
+        pl.semaphore_signal(barrier, inc=1, device_id=dev, device_id_type=MESH)
+
+    load_r.wait()
+    load_w.wait()
 
     r0 = routes_ref[0:1, :]
     r1 = routes_ref[1:2, :]
@@ -153,26 +173,54 @@
         zz, hh = to_of(p)
         return remote(
             sendbuf.at[a, rows_of(zz * 2 + hh)], place_of(a, p),
-            a2a_send.at[a, p], a2a_recv.at[a, p], holder(zz, hh),
+            a2a_send.at[a], a2a_recv.at[a, p // 8], holder(zz, hh),
         )
 
     def a2a_wait(a, h):
-        for p in range(8 * h, 8 * h + 8):
-            if p == 0:
-                own[a].wait()
-            else:
-                out_copy(a, p).wait_recv()
+        if h == 0:
+            own[a].wait()
+        all_in(xc.at[a, h, m_own, y, pl.ds(0, 112 + 16 * h)], a2a_recv.at[a, h])
+
+    def far_copy(a, p):
+        zz, hh = to_of(p)
+        return remote(
+            sendbuf2.at[a, rows_of(zz * 2 + hh)], xc.at[a, 0, m_own, y2, pl.ds(p * 16, 16)],
+            far_send.at[a], far_recv.at[a], holder(zz, hh),
+        )
 
     own = [
         pltpu.make_async_copy(sendbuf.at[a, rows_of(me)], place_of(a, 0), own_sem.at[a])
         for a in range(2)
     ]
-    for h in range(2):
+    own2 = [
+        pltpu.make_async_copy(
+            sendbuf2.at[a, rows_of(me)], xc.at[a, 0, m_own, y2, pl.ds(0, 16)], own_sem.at[2 + a]
+        )
+        for a in range(2)
+    ]
+
+    def push(h):
         for a in range(2):
-            if h == 0:
-                own[a].start()
-            for p in range(max(8 * h, 1), 8 * h + 8):
-                out_copy(a, p).start()
+            for p in reversed(range(8 * h, 8 * h + 8)):
+                if p == 0:
+                    own[a].start()
+                else:
+                    out_copy(a, p).start()
+
+    def push_far(a):
+        for p in reversed(range(1, 8)):
+            far_copy(a, p).start()
+        own2[a].start()
+
+    def far_wait(a):
+        own2[a].wait()
+        all_in(xc.at[a, 0, m_own, y2, pl.ds(0, 112)], far_recv.at[a])
+
+    push(0)
+    load_far[0].wait()
+    sendbuf2[0] = mm(perm_val, xq2[...], NN).astype(BF)
+    load_far[1].wait()
+    sendbuf2[1] = (w_slot * mm(perm_val, cq2[...], NN)).astype(BF)
 
     lane = lax.broadcasted_iota(jnp.int32, (128, 128), 1)
 
@@ -181,14 +229,13 @@
         st_out[phase] = cols2.T[0:8, :]
         return [
             remote(
-                st_out.at[phase], st_in.at[phase, j], st_send.at[phase, j], st_recv.at[phase, j], dev
+                st_out.at[phase], st_in.at[phase, j], st_send.at[phase], st_recv.at[phase], dev
             )
             for j, dev in enumerate((dev_p, dev_m, dev_2))
         ]
 
-    def sums_in(phase, copies):
-        for copy in copies:
-            copy.wait_recv()
+    def sums_in(phase):
+        all_in(st_in.at[phase], st_recv.at[phase])
         tot = (st_out[phase] + st_in[phase, 2]) + (st_in[phase, 0] + st_in[phase, 1])
         tall = jnp.concatenate([tot, jnp.zeros((120, 128), F32)], axis=0).T
         return tall[:, 0:1], tall[:, 1:2]
@@ -210,7 +257,12 @@
         return xc.at[a, h, gg * 2 + cc, yy]
 
     def ag_copy(a, h, kind, ref, dev):
-        return remote(ref, ref, ag_send.at[a * 2 + h, kind], ag_recv.at[a * 2 + h, kind], dev)
+        lot = 4 if kind in (3, 4) else 8 if kind >= 8 else 0
+        slot = kind if kind < 8 else 5 + kind // 4
+        slot = slot + 1 if kind >= 8 else slot
+        return remote(
+            ref, ref, ag_send.at[a * 2 + h + lot], ag_recv.at[a * 2 + h, slot], dev
+        )
 
     def ag_out(a, h, kind):
         if kind >= 8:
@@ -252,18 +304,24 @@
         for kind in kinds:
             ag_in(a, h, kind).wait_recv()
 
+    def sib_got(a, h, gg):
+        all_in(xc.at[a, h, gg * 2 + oc], ag_recv.at[a * 2 + h, 8 if gg is g else 9])
+
     def relay_y(a, h):
         got(a, h, 1)
-        go(a, h, 3, 9)
+        go(a, h, *((3, 9) if h else (9,)))
         got(a, h, 2)
-        go(a, h, 4, 10)
+        go(a, h, *((4, 10) if h else (10,)))
 
     def relay_x(a, h):
         got(a, h, 0)
         go(a, h, 5, 6, 12)
 
     def relay_far(a, h):
-        got(a, h, 3, 4)
+        if h:
+            got(a, h, 3, 4)
+        else:
+            far_wait(a)
         go(a, h, 7, 11)
 
     def relay_last(a, h):
@@ -280,24 +338,26 @@
     def rows_at(a, h, gg, q):
         return xc[a, h, pair(gg), q].reshape(256, 512)
 
-    def forward(h, gg):
+    def pre_acts(h, gg):
         pre_g = jnp.zeros((256, 224), F32)
         pre_u = jnp.zeros((256, 224), F32)
-        d_act = jnp.zeros((256, 224), F32)
         for q in range(4):
             span = slice(q * 512, q * 512 + 512)
             rows = rows_at(0, h, gg, q)
             pre_g += mm(rows, wg[:, span], NT)
             pre_u += mm(rows, wu[:, span], NT)
+        return pre_g, pre_u
+
+    def forward(h, gg, pres):
+        pre_g, pre_u = pres
+        d_act = jnp.zeros((256, 224), F32)
+        for q in range(4):
+            span = slice(q * 512, q * 512 + 512)
             d_act += mm(rows_at(1, h, gg, q), wd[:, span], NT)
         sig = jax.nn.sigmoid(pre_g)
         d_gate = (d_act * pre_u * swish_slope(pre_g, sig)).astype(BF)
         d_up = (d_act * pre_g * sig).astype(BF)
-        slot = h * 2 + gg
-        act_t[slot] = (pre_g * sig * pre_u).T.astype(BF)
-        dg_t[slot] = d_gate.T
-        du_t[slot] = d_up.T
-        return d_gate, d_up
+        return d_gate, d_up, pre_g * sig * pre_u
 
     def back(h, gg, grads, yy):
         span = pl.ds(pl.multiple_of(yy * 512, 512), 512)
@@ -310,16 +370,20 @@
         at = (0 if gg is g else 4) + j
         return remote(
             part.at[h, gg * 2 + oc, order[j]], sib_in.at[h, gg, order[j]],
-            sb_send.at[h, at], sb_recv.at[h, at], dev_s,
+            sb_send.at[h], sb_recv.at[h, at], dev_s,
         )
 
-    def whole(h, gg, *between):
-        grads = forward(h, gg)
+    def whole(h, gg, pres, *between):
+        grads = forward(h, gg, pres)
         for j in range(4):
             back(h, gg, grads, order[j])
             sib_copy(h, gg, j).start()
             if j < len(between):
                 between[j]()
+        slot = h * 2 + gg
+        act_t[slot] = grads[2].T.astype(BF)
+        dg_t[slot] = grads[0].T
+        du_t[slot] = grads[1].T
 
     m_g, m_o = g * 2 + c, og * 2 + c
 
@@ -328,36 +392,54 @@
         at = (h, gg * 2 + c, order[j])
         part[at] = (part[at].astype(F32) + sib_in[h, gg, order[j]].astype(F32)).astype(BF)
 
+    def pieces(h):
+        n = 1 + h
+        return n, [i for k in range(n) for i in (k, n + k)]
+
+    def piece(h, i):
+        rows = 64 // (1 + h)
+        return pl.ds(i * rows, rows)
+
     def rs_copy(h, kind):
-        src, dst, dev = (
-            (part.at[h, m_o, y2, first], in_a.at[h, first], dev_x),
-            (part.at[h, m_o, y2, second], in_a.at[h, second], dev_x),
-            (part.at[h, m_o, yp], in_b.at[h, 0], dev_p),
-            (part.at[h, m_o, ym], in_b.at[h, 1], dev_m),
-            (part.at[h, m_g, y2, first], in_c.at[h, 0], dev_p),
-            (part.at[h, m_g, y2, second], in_c.at[h, 1], dev_m),
-            (part.at[h, m_o, y], in_d.at[h], dev_x),
-            (part.at[h, m_g, yp, second], in_e.at[h, 0, second], dev_p),
-            (part.at[h, m_g, ym, first], in_e.at[h, 1, first], dev_m),
-            (part.at[h, m_g, yp, first], in_e.at[h, 0, first], dev_p),
-            (part.at[h, m_g, ym, second], in_e.at[h, 1, second], dev_m),
-        )[kind]
-        return remote(src, dst, rs_send.at[h, kind], rs_recv.at[h, kind], dev)
+        n = 1 + h
+        if kind < 4:
+            at = piece(h, kind)
+            src, dst, dev = part.at[h, m_o, y2, at], in_a.at[h, at], dev_x
+        elif kind < 8:
+            at = piece(h, kind - 4)
+            src, dst = part.at[h, m_g, y2, at], in_c.at[h, at]
+            dev = dev_p if kind - 4 < n else dev_m
+        elif kind < 12:
+            at = piece(h, kind - 8)
+            yy, i, dev = (yp, 0, dev_p) if kind - 8 < n else (ym, 1, dev_m)
+            src, dst = part.at[h, m_g, yy, at], in_e.at[h, i, at]
+        else:
+            src, dst, dev = (
+                (part.at[h, m_o, yp], in_b.at[h, 0], dev_p),
+                (part.at[h, m_o, ym], in_b.at[h, 1], dev_m),
+                (part.at[h, m_o, y], in_d.at[h], dev_x),
+                (part.at[h, m_g, yp, second], in_e.at[h, 0, second], dev_p),
+                (part.at[h, m_g, ym, first], in_e.at[h, 1, first], dev_m),
+            )[kind - 12]
+        slot = kind if kind < 8 else 8 if kind in (12, 13) else 9
+        lot = 0 if 4 <= kind < 8 or 12 <= kind < 15 else 1
+        return remote(src, dst, rs_send.at[h, lot], rs_recv.at[h, slot], dev)
 
     def rs_open(h):
         pair_sum(h, og, 0)
-        rs_copy(h, 0).start()
-        rs_copy(h, 1).start()
+        for i in pieces(h)[1]:
+            rs_copy(h, i).start()
         pair_sum(h, og, 1)
-        rs_copy(h, 2).start()
+        rs_copy(h, 12).start()
         pair_sum(h, og, 2)
-        rs_copy(h, 3).start()
+        rs_copy(h, 13).start()
 
     def rs_own(h):
-        for j, kind in ((1, 7), (2, 8), (0, None)):
-            pair_sum(h, g, j)
-            if kind:
-                rs_copy(h, kind).start()
+        pair_sum(h, g, 1)
+        rs_copy(h, 15).start()
+        pair_sum(h, g, 2)
+        rs_copy(h, 16).start()
+        pair_sum(h, g, 0)
         pair_sum(h, og, 3)
         pair_sum(h, g, 3)
 
@@ -368,50 +450,45 @@
         part[at] = value.astype(BF)
 
     def rs_far(h):
-        rs_copy(h, 0).wait_recv()
-        add_to((h, m_g, y2, first), in_a[h, first])
-        rs_copy(h, 4).start()
-        rs_copy(h, 1).wait_recv()
-        add_to((h, m_g, y2, second), in_a[h, second])
-        rs_copy(h, 5).start()
+        for i in pieces(h)[1]:
+            rs_copy(h, i).wait_recv()
+            add_to((h, m_g, y2, piece(h, i)), in_a[h, piece(h, i)])
+            rs_copy(h, 4 + i).start()
 
     def rs_cross(h):
-        rs_copy(h, 2).wait_recv()
-        rs_copy(h, 3).wait_recv()
+        all_in(in_b.at[h], rs_recv.at[h, 8])
         add_to((h, m_o, y), in_b[h, 0], in_b[h, 1])
-        rs_copy(h, 6).start()
+        rs_copy(h, 14).start()
 
     def rs_near(h):
-        rs_copy(h, 4).wait_recv()
-        add_to((h, m_g, yp, first), in_c[h, 0])
-        rs_copy(h, 9).start()
-        rs_copy(h, 5).wait_recv()
-        add_to((h, m_g, ym, second), in_c[h, 1])
-        rs_copy(h, 10).start()
+        n, turns = pieces(h)
+        for i in turns:
+            rs_copy(h, 4 + i).wait_recv()
+            add_to((h, m_g, yp if i < n else ym, piece(h, i)), in_c[h, piece(h, i)])
+            rs_copy(h, 8 + i).start()
 
     def ret_copy(p):
         zz, hh = from_of(p)
         return remote(
             total.at[p // 8, pl.ds(p % 8 * 16, 16)], ret.at[rows_of(me)],
-            ret_send.at[p], ret_recv.at[p], holder(zz, hh),
+            ret_send.at[0], ret_recv.at[0], holder(zz, hh),
         )
 
     own_back = pltpu.make_async_copy(total.at[0, pl.ds(0, 16)], ret.at[rows_of(me)], own_sem.at[0])
 
     def rs_close(h):
-        for kind in range(6, 11):
-            rs_copy(h, kind).wait_recv()
+        all_in(part.at[h, 0, pl.ds(0, 3)], rs_recv.at[h, 9])
         total[h] = (
             part[h, m_g, y].astype(F32) + in_d[h].astype(F32)
             + in_e[h, 0].astype(F32) + in_e[h, 1].astype(F32)
         ).astype(BF)
-        for p in range(8 * h, 8 * h + 8):
+        for p in reversed(range(8 * h, 8 * h + 8)):
             if p == 0:
                 own_back.start()
             else:
                 ret_copy(p).start()
 
-    def weight_grad(out_ref, source, a):
+    def weight_grad(out_ref, source, a, half):
         def tile(q, _):
             acc = jnp.zeros((source.shape[1], 512), F32)
             for h in range(2):
@@ -420,19 +497,38 @@
             out_ref[:, pl.ds(pl.multiple_of(q * 512, 512), 512)] = acc.astype(BF)
             return 0
 
-        lax.fori_loop(0, 4, tile, 0)
+        lax.fori_loop(2 * half, 2 * half + 2, tile, 0)
+
+    def drain_rows(a):
+        all_sent(sendbuf.at[a, pl.ds(0, 240)], a2a_send.at[a])
+        all_sent(sendbuf2.at[a, pl.ds(0, 112)], far_send.at[a])
+        for h in range(2):
+            all_sent(xc.at[a, h, pl.ds(0, 2), pl.ds(0, 3)], ag_send.at[a * 2 + h])
+            all_sent(xc.at[a, h, pl.ds(0, 2)], ag_send.at[a * 2 + h + 8])
+        all_sent(xc.at[a, 1, 0, 0], ag_send.at[a * 2 + 5])
+
+    def drain_sums():
+        for h in range(2):
+            all_sent(part.at[h, pl.ds(0, 2)], sb_send.at[h])
+            all_sent(part.at[h, 0], rs_send.at[h, 0])
+            all_sent(part.at[h, 0, pl.ds(0, 3)], rs_send.at[h, 1])
 
     a2a_wait(0, 0)
     go(0, 0, 0, 1, 2, 8)
+    push_far(0)
+    push_far(1)
+    push(1)
     a2a_wait(1, 0)
     go(1, 0, 0, 1, 2, 8)
+    relay_x(0, 0)
+    relay_x(1, 0)
     relay_y(0, 0)
     relay_y(1, 0)
-    relay_x(0, 0)
-    relay_x(1, 0)
+    relay_far(0, 0)
+    relay_far(1, 0)
     a2a_wait(0, 1)
     go(0, 1, 0, 1, 2, 8)
-    sum1, sum2 = sums_in(0, stats)
+    sum1, sum2 = sums_in(0)
     mean = sum1 / DB
     rstd = lax.rsqrt(sum2 / DB - mean * mean + 1e-05)
     norm_val = (conv_ref[...].astype(F32) - mean) * rstd
@@ -442,49 +538,56 @@
     mixed[...] = (zpre * zsig).astype(BF)
     slope[...] = swish_slope(zpre, zsig) * gain_ref[...]
     scale[...] = jnp.broadcast_to(rstd, (128, 256))
-    relay_far(0, 0)
-    relay_far(1, 0)
+    for copy in loads:
+        copy.wait()
+    sib_got(0, 0, g)
+    pres = pre_acts(0, g)
     a2a_wait(1, 1)
     go(1, 1, 0, 1, 2, 8)
-    for copy in loads:
-        copy.wait()
-    got(0, 0, 8, 9, 10, 11)
-    got(1, 0, 8, 9, 10, 11)
-    whole(0, g)
+    sib_got(1, 0, g)
+    whole(0, g, pres)
     relay_last(0, 0)
     relay_last(1, 0)
     relay_y(0, 1)
-    got(0, 0, 12, 13, 14, 15)
-    got(1, 0, 12, 13, 14, 15)
-    whole(0, og, lambda: relay_y(1, 1), lambda: relay_x(0, 1), lambda: relay_x(1, 1))
+    sib_got(0, 0, og)
+    pres = pre_acts(0, og)
+    sib_got(1, 0, og)
+    relay_x(0, 1)
+    relay_y(1, 1)
+    whole(0, og, pres, lambda: relay_x(1, 1), lambda: relay_far(0, 1))
+    sib_got(0, 1, g)
+    pres = pre_acts(1, g)
+    relay_far(1, 1)
+    sib_got(1, 1, g)
+    whole(1, g, pres)
     rs_open(0)
+    relay_last(0, 1)
     rs_own(0)
-    relay_far(0, 1)
-    relay_far(1, 1)
-    got(0, 1, 8, 9, 10, 11)
-    got(1, 1, 8, 9, 10, 11)
-    whole(1, g)
-    rs_far(0)
-    relay_last(0, 1)
+    sib_got(0, 1, og)
+    pres = pre_acts(1, og)
     relay_last(1, 1)
-    got(0, 1, 12, 13, 14, 15)
-    got(1, 1, 12, 13, 14, 15)
-    whole(1, og)
+    sib_got(1, 1, og)
+    whole(1, og, pres, lambda: rs_far(0))
     rs_open(1)
     rs_cross(0)
     rs_own(1)
+    drain_rows(0)
     rs_near(0)
-    weight_grad(gg_ref, dg_t, 0)
-    weight_grad(gu_ref, du_t, 0)
+    weight_grad(gg_ref, dg_t, 0, 0)
+    weight_grad(gg_ref, dg_t, 0, 1)
     rs_far(1)
+    weight_grad(gu_ref, du_t, 0, 0)
     rs_cross(1)
+    weight_grad(gu_ref, du_t, 0, 1)
+    drain_rows(1)
     rs_near(1)
     rs_close(0)
-    weight_grad(gd_ref, act_t, 1)
+    weight_grad(gd_ref, act_t, 1, 0)
+    weight_grad(gd_ref, act_t, 1, 1)
     rs_close(1)
-
-    for p in range(1, 16):
-        ret_copy(p).wait_recv()
+    drain_sums()
+
+    all_in(ret.at[pl.ds(0, 240)], ret_recv.at[0])
     own_back.wait()
     moe = mm(perm[...], ret[...], TN)
     res_ref[y] = (cq[...].astype(F32) + moe).astype(BF)
@@ -492,7 +595,7 @@
     half0, half1 = pl.ds(0, 64), pl.ds(64, 64)
 
     def res_copy(kind, ref, dev):
-        return remote(ref, ref, res_send.at[kind], res_recv.at[kind], dev)
+        return remote(ref, ref, res_send.at[0], res_recv.at[kind], dev)
 
     def res_out(kind):
         ref, dev = (
@@ -520,7 +623,7 @@
 
     def gp_copy(q, j):
         return remote(
-            gp.at[oc, :, pair_of(q)], gp_sib.at[:, pair_of(q)], gs_send.at[j], gs_recv.at[j], dev_s
+            gp.at[oc, :, pair_of(q)], gp_sib.at[:, pair_of(q)], gs_send.at[0], gs_recv.at[j], dev_s
         )
 
     def proj_terms(q, j):
@@ -535,7 +638,7 @@
     def gx_copy(q, j, i):
         return remote(
             gp.at[c, others_x[i], pair_of(q)], gp_x.at[i, pair_of(q)],
-            gx_send.at[j, i], gx_recv.at[j, i], at_x(others_x[i]),
+            gx_send.at[0], gx_recv.at[j], at_x(others_x[i]),
         )
 
     def over_x(q, j):
@@ -547,12 +650,11 @@
             gx_copy(q, j, i).start()
 
     def gz_copy(to, slot):
-        return remote(gp_row.at[to], gp_z.at[slot], gz_send.at[to], gz_recv.at[slot], at_z(to))
+        return remote(gp_row.at[to], gp_z.at[slot], gz_send.at[0], gz_recv.at[0], at_z(to))
 
     def over_z(q, j):
-        for i in range(3):
-            gx_copy(q, j, i).wait_recv()
         pair = pair_of(q)
+        all_in(gp_x.at[:, pair], gx_recv.at[j])
         gp_row[pair] = (
             (gp[c, x, pair].astype(F32) + gp_x[0, pair].astype(F32))
             + (gp_x[1, pair].astype(F32) + gp_x[2, pair].astype(F32))
@@ -589,10 +691,8 @@
         copy.start()
     over_x(y2, 3)
     over_z(y, 0)
-    over_z(ym, 1)
-    over_z(yp, 2)
-
-    first_sum, second_sum = sums_in(1, stats2)
+
+    first_sum, second_sum = sums_in(1)
     conv_grad = (
         scale[...] * (d_norm - first_sum / DB - norm_val * (second_sum / DB))
     ).astype(BF)
@@ -600,6 +700,8 @@
     halo = remote(halo_out, halo_in, halo_sem.at[0], halo_sem.at[1], dev_prev)
     halo.start()
     ext[0:128, :] = conv_grad.astype(F32)
+    over_z(ym, 1)
+    over_z(yp, 2)
 
     def correlate(start, count):
         acc = jnp.zeros((count, 256), F32)
@@ -624,37 +726,21 @@
     ext[128:160, :] = halo_in[...].astype(F32) * keep
     glu_grads(96, 32, correlate(96, 32))
 
+    all_in(gp_z.at[pl.ds(0, 7)], gz_recv.at[0])
     rows_sum = gp_row[z].astype(F32)
     for k in range(1, 8):
         zz = lax.rem(z + k, 8)
-        gz_copy(zz, zz).wait_recv()
         rows_sum += gp_z[zz].astype(F32)
     gp_ref[...] = rows_sum
 
-    for a in range(2):
-        for p in range(1, 16):
-            out_copy(a, p).wait_send()
-        for h in range(2):
-            for kind in range(16):
-                ag_out(a, h, kind).wait_send()
-    for h in range(2):
-        for gg in (g, og):
-            for j in range(4):
-                sib_copy(h, gg, j).wait_send()
-        for kind in range(11):
-            rs_copy(h, kind).wait_send()
-    for p in range(1, 16):
-        ret_copy(p).wait_send()
-    for copy in (*stats, *stats2, halo):
-        copy.wait_send()
-    for kind in range(6):
-        res_out(kind).wait_send()
-    for j, q in enumerate((y, ym, yp, y2)):
-        gp_copy(q, j).wait_send()
-        for i in range(3):
-            gx_copy(q, j, i).wait_send()
-    for k in range(1, 8):
-        gz_copy(lax.rem(z + k, 8), z).wait_send()
+    all_sent(ret.at[pl.ds(0, 240)], ret_send.at[0])
+    for phase in range(2):
+        all_sent(st_in.at[phase], st_send.at[phase])
+    halo.wait_send()
+    all_sent(res_ref.at[pl.ds(0, 3)], res_send.at[0])
+    all_sent(gp.at[oc], gs_send.at[0])
+    all_sent(gp_x, gx_send.at[0])
+    all_sent(gp_z.at[pl.ds(0, 7)], gz_send.at[0])
 
 
 def write_kernel(*refs):
@@ -691,12 +777,15 @@
     results = pl.pallas_call(
         backward_kernel,
         out_shape=[pltpu.VMEM(a.shape, a.dtype) for a in shapes],
-        in_specs=[vmem] * 3 + [hbm] * 10,
+        in_specs=[vmem] + [hbm] * 12,
         out_specs=[vmem] * 6,
         scratch_shapes=[
             pltpu.VMEM((128, 512), BF),
             pltpu.VMEM((128, 512), BF),
+            pltpu.VMEM((128, 512), BF),
+            pltpu.VMEM((128, 512), BF),
             pltpu.VMEM((256, 128), BF),
+            pltpu.VMEM((2, 256, 512), BF),
             pltpu.VMEM((2, 256, 512), BF),
             pltpu.VMEM((2, 2, 4, 4, 128, 512), BF),
             pltpu.VMEM((units, width), BF),
@@ -709,11 +798,13 @@
             pltpu.VMEM((2, 2, 4, 128, 512), BF),
             pltpu.VMEM((2, 128, 512), BF),
             pltpu.VMEM((2, 2, 128, 512), BF),
-            pltpu.VMEM((2, 2, 64, 512), BF),
+            pltpu.VMEM((2, 128, 512), BF),
             pltpu.VMEM((2, 128, 512), BF),
             pltpu.VMEM((2, 2, 128, 512), BF),
             pltpu.VMEM((2, 128, 512), BF),
             pltpu.VMEM((256, 512), BF),
+            pltpu.VMEM((2, tokens), jnp.int32),
+            pltpu.VMEM((2, tokens), F32),
             pltpu.VMEM((tokens, channels), BF),
             pltpu.VMEM((tokens, channels), BF),
             pltpu.VMEM((tokens, channels), BF),
@@ -734,19 +825,19 @@
             pltpu.VMEM((3, 8, 32, 256), BF),
             pltpu.VMEM((8, 32, 256), BF),
             pltpu.VMEM((8, 32, 256), BF),
-            dma((10,)), dma((2,)),
-            dma((2, 16)), dma((2, 16)), dma((4, 16)), dma((4, 16)),
-            dma((2, 8)), dma((2, 8)), dma((2, 11)), dma((2, 11)),
-            dma((16,)), dma((16,)), dma((6,)), dma((6,)),
-            dma((2, 3)), dma((2, 3)), dma((2,)),
-            dma((4,)), dma((4,)), dma((4, 3)), dma((4, 3)), dma((8,)), dma((8,)),
+            dma((14,)), dma((4,)),
+            dma((2,)), dma((2, 2)), dma((2,)), dma((2,)), dma((12,)), dma((4, 10)),
+            dma((2,)), dma((2, 8)), dma((2, 2)), dma((2, 10)),
+            dma((1,)), dma((1,)), dma((1,)), dma((6,)),
+            dma((2,)), dma((2,)), dma((2,)),
+            dma((1,)), dma((4,)), dma((1,)), dma((4,)), dma((1,)), dma((1,)),
         ],
         compiler_params=pltpu.CompilerParams(
             collective_id=0, has_side_effects=True, vmem_limit_bytes=60 * 1024 * 1024
         ),
         name="backward",
     )(
-        routes.T, route_weight.T, norm_gain[None, :],
+        norm_gain[None, :], routes.T, route_weight.T,
         moe_input, out_cotangent, w_gate[0].T, w_up[0].T, w_down[0], out_proj,
         conv_out, glu_value, glu_gate, taps,
     )

time: 97.7 us -> 92.3 us (0.945)
  Pallas kernels: 96.8 us -> 91.4 us
    pallas_call x1, Pallas kernels: 95.2 us -> 89.7 us  [local(): pl.pallas_call(backward_kernel, out_shape=[pltpu.VMEM(a.shape, a.dtype) f...]
where the time goes in v5:
time: 92.3 us; the launch traced here: 92.2 us
  Pallas kernels  91.4 us (99%)
    pallas_call x1, Pallas kernels, local(): pl.pallas_call(backward_kernel, out_shape=[pltpu.VMEM(a.shape, a.dtype) f...  89.7 us

profile of v5, /device:TPU:16, one launch (start us, length us, event | category | flops | bytes accessed | tf_op | source)
XLA Modules:
  0.0 92.2 jit_solution(16483228840574214856)
XLA Ops:
  0.6 89.7 %backward.1 = (bf16[224,2048]{1,0:T(8,128)(2,1)S(1)}, bf16[224,2048]{1,0:T(8,128)(2,1)S(1)}, bf16[224,2048]{1,0:T(8,128)(2,1)S(1)}, f32[32,256]{1,0:T(8,128)S(1)...) custom-call(f32[1,256]{1,0:T(1,128)} %bitcast.20, s32[2,128]{1,0:T(2,128)} %bitcast.21, f32[2,128]{1,0:T(2,128)} %bitcast.22, ...), custom_call_target="tpu_custom_call" | custom-call | tf_op jit(solution)/shard_map/backward/pallas_call | solution.py:777
  90.4 1.6 %write_out.1 = (bf16[224,2048]{1,0:T(8,128)(2,1)}, bf16[224,2048]{1,0:T(8,128)(2,1)}, bf16[224,2048]{1,0:T(8,128)(2,1)}, f32[32,256]{1,0:T(8,128)}, bf16[128,256]{1,0:T(8,128)(2,1)}, /*index=5*/bf16[128,256]{1,0:T(8,128)(2,1)}) custom-call(bf16[224,2048]{1,0:T(8,128)(2,1)S(1)} %get-tuple-element.18.refs_0_, bf16[224,2048]{1,0:T(8,128)(2,1)S(1)} %get-tuple-element.19.refs_1_, ...), custom_call_target="tpu_custom_call" | custom-call | tf_op jit(solution)/shard_map/write_out/pallas_call | solution.py:844

commit v6 on v5

--- a/solution.py
+++ b/solution.py
@@ -378,7 +378,7 @@
         for j in range(4):
             back(h, gg, grads, order[j])
             sib_copy(h, gg, j).start()
-            if j < len(between):
+            if j < len(between) and between[j]:
                 between[j]()
         slot = h * 2 + gg
         act_t[slot] = grads[2].T.astype(BF)
@@ -415,33 +415,42 @@
             src, dst = part.at[h, m_g, yy, at], in_e.at[h, i, at]
         else:
             src, dst, dev = (
-                (part.at[h, m_o, yp], in_b.at[h, 0], dev_p),
-                (part.at[h, m_o, ym], in_b.at[h, 1], dev_m),
-                (part.at[h, m_o, y], in_d.at[h], dev_x),
+                (part.at[h, m_o, yp, first], in_b.at[h, 0, first], dev_p),
+                (part.at[h, m_o, ym, first], in_b.at[h, 1, first], dev_m),
+                (part.at[h, m_o, y, first], in_d.at[h, first], dev_x),
                 (part.at[h, m_g, yp, second], in_e.at[h, 0, second], dev_p),
                 (part.at[h, m_g, ym, first], in_e.at[h, 1, first], dev_m),
+                (part.at[h, m_o, yp, second], in_b.at[h, 0, second], dev_p),
+                (part.at[h, m_o, ym, second], in_b.at[h, 1, second], dev_m),
+                (part.at[h, m_o, y, second], in_d.at[h, second], dev_x),
             )[kind - 12]
-        slot = kind if kind < 8 else 8 if kind in (12, 13) else 9
-        lot = 0 if 4 <= kind < 8 or 12 <= kind < 15 else 1
+        slot = kind if kind < 8 else 8 if kind in (12, 13) else 10 if kind in (17, 18) else 9
+        lot = 0 if kind in (4, 5, 6, 7, 12, 13, 14, 17, 18, 19) else 1
         return remote(src, dst, rs_send.at[h, lot], rs_recv.at[h, slot], dev)
 
-    def rs_open(h):
+    def rs_chain(h):
         pair_sum(h, og, 0)
         for i in pieces(h)[1]:
             rs_copy(h, i).start()
+
+    def rs_open(h):
         pair_sum(h, og, 1)
         rs_copy(h, 12).start()
+        rs_copy(h, 17).start()
         pair_sum(h, og, 2)
         rs_copy(h, 13).start()
+        rs_copy(h, 18).start()
 
     def rs_own(h):
         pair_sum(h, g, 1)
-        rs_copy(h, 15).start()
         pair_sum(h, g, 2)
-        rs_copy(h, 16).start()
         pair_sum(h, g, 0)
         pair_sum(h, og, 3)
         pair_sum(h, g, 3)
+
+    def rs_early(h):
+        rs_copy(h, 15).start()
+        rs_copy(h, 16).start()
 
     def add_to(at, *terms):
         value = part[at].astype(F32)
@@ -455,10 +464,11 @@
             add_to((h, m_g, y2, piece(h, i)), in_a[h, piece(h, i)])
             rs_copy(h, 4 + i).start()
 
-    def rs_cross(h):
-        all_in(in_b.at[h], rs_recv.at[h, 8])
-        add_to((h, m_o, y), in_b[h, 0], in_b[h, 1])
-        rs_copy(h, 14).start()
+    def rs_cross(h, half):
+        at = (first, second)[half]
+        all_in(in_b.at[h, :, at], rs_recv.at[h, 8 + 2 * half])
+        add_to((h, m_o, y, at), in_b[h, 0, at], in_b[h, 1, at])
+        rs_copy(h, 14 + 5 * half).start()
 
     def rs_near(h):
         n, turns = pieces(h)
@@ -552,38 +562,43 @@
     sib_got(0, 0, og)
     pres = pre_acts(0, og)
     sib_got(1, 0, og)
+    relay_y(1, 1)
     relay_x(0, 1)
-    relay_y(1, 1)
-    whole(0, og, pres, lambda: relay_x(1, 1), lambda: relay_far(0, 1))
+    whole(0, og, pres, lambda: relay_far(0, 1), lambda: relay_x(1, 1))
     sib_got(0, 1, g)
     pres = pre_acts(1, g)
     relay_far(1, 1)
+    rs_chain(0)
+    rs_open(0)
     sib_got(1, 1, g)
     whole(1, g, pres)
-    rs_open(0)
+    rs_own(0)
+    rs_early(0)
     relay_last(0, 1)
-    rs_own(0)
     sib_got(0, 1, og)
+    relay_last(1, 1)
     pres = pre_acts(1, og)
-    relay_last(1, 1)
     sib_got(1, 1, og)
-    whole(1, og, pres, lambda: rs_far(0))
+    whole(1, og, pres, lambda: rs_far(0), None, lambda: rs_chain(1))
     rs_open(1)
-    rs_cross(0)
     rs_own(1)
+    weight_grad(gg_ref, dg_t, 0, 0)
+    rs_cross(0, 0)
+    rs_cross(0, 1)
     drain_rows(0)
-    rs_near(0)
-    weight_grad(gg_ref, dg_t, 0, 0)
     weight_grad(gg_ref, dg_t, 0, 1)
     rs_far(1)
+    rs_early(1)
+    rs_near(0)
+    rs_cross(1, 0)
     weight_grad(gu_ref, du_t, 0, 0)
-    rs_cross(1)
+    rs_cross(1, 1)
     weight_grad(gu_ref, du_t, 0, 1)
+    rs_near(1)
+    weight_grad(gd_ref, act_t, 1, 0)
     drain_rows(1)
-    rs_near(1)
+    weight_grad(gd_ref, act_t, 1, 1)
     rs_close(0)
-    weight_grad(gd_ref, act_t, 1, 0)
-    weight_grad(gd_ref, act_t, 1, 1)
     rs_close(1)
     drain_sums()
 
@@ -592,29 +607,16 @@
     moe = mm(perm[...], ret[...], TN)
     res_ref[y] = (cq[...].astype(F32) + moe).astype(BF)
 
-    half0, half1 = pl.ds(0, 64), pl.ds(64, 64)
-
-    def res_copy(kind, ref, dev):
+    def slab(i):
+        return pl.ds(i * 32, 32)
+
+    def res_copy(yy, i, kind, dev):
+        ref = res_ref.at[yy, slab(i)]
         return remote(ref, ref, res_send.at[0], res_recv.at[kind], dev)
 
-    def res_out(kind):
-        ref, dev = (
-            (res_ref.at[y, half0], dev_p), (res_ref.at[y, half1], dev_p),
-            (res_ref.at[y, half1], dev_m), (res_ref.at[y, half0], dev_m),
-            (res_ref.at[ym, half0], dev_p), (res_ref.at[yp, half1], dev_m),
-        )[kind]
-        return res_copy(kind, ref, dev)
-
-    def res_in(kind):
-        ref, dev = (
-            (res_ref.at[ym, half0], dev_m), (res_ref.at[ym, half1], dev_m),
-            (res_ref.at[yp, half1], dev_p), (res_ref.at[yp, half0], dev_p),
-            (res_ref.at[y2, half0], dev_m), (res_ref.at[y2, half1], dev_p),
-        )[kind]
-        return res_copy(kind, ref, dev)
-
-    for kind in (0, 2, 1, 3):
-        res_out(kind).start()
+    for i in range(4):
+        res_copy(y, i, min(i, 2), dev_p).start()
+        res_copy(y, 3 - i, 3 + min(i, 2), dev_m).start()
     for copy in late_loads:
         copy.wait()
 
@@ -666,19 +668,20 @@
                 gz_copy(q * 2 + i, z).start()
 
     d_mixed = proj_terms(y, 0)
-    res_in(0).wait_recv()
-    res_out(4).start()
-    res_in(2).wait_recv()
-    res_out(5).start()
+    for i in range(2):
+        res_copy(ym, i, i, dev_m).wait_recv()
+        res_copy(ym, i, 6, dev_p).start()
+        res_copy(yp, 3 - i, 3 + i, dev_p).wait_recv()
+        res_copy(yp, 3 - i, 7, dev_m).start()
     over_x(y, 0)
-    res_in(1).wait_recv()
+    all_in(res_ref.at[ym, pl.ds(64, 64)], res_recv.at[2])
     d_mixed += proj_terms(ym, 1)
-    res_in(3).wait_recv()
+    all_in(res_ref.at[yp, pl.ds(0, 64)], res_recv.at[5])
     d_mixed += proj_terms(yp, 2)
     over_x(ym, 1)
     over_x(yp, 2)
-    res_in(4).wait_recv()
-    res_in(5).wait_recv()
+    all_in(res_ref.at[y2, pl.ds(0, 64)], res_recv.at[6])
+    all_in(res_ref.at[y2, pl.ds(64, 64)], res_recv.at[7])
     d_mixed += proj_terms(y2, 3)
     d_norm = d_mixed * slope[...]
     norm_val = normed[...]
@@ -827,8 +830,8 @@
             pltpu.VMEM((8, 32, 256), BF),
             dma((14,)), dma((4,)),
             dma((2,)), dma((2, 2)), dma((2,)), dma((2,)), dma((12,)), dma((4, 10)),
-            dma((2,)), dma((2, 8)), dma((2, 2)), dma((2, 10)),
-            dma((1,)), dma((1,)), dma((1,)), dma((6,)),
+            dma((2,)), dma((2, 8)), dma((2, 2)), dma((2, 11)),
+            dma((1,)), dma((1,)), dma((1,)), dma((8,)),
             dma((2,)), dma((2,)), dma((2,)),
             dma((1,)), dma((4,)), dma((1,)), dma((4,)), dma((1,)), dma((1,)),
         ],

time: 92.3 us -> 89.1 us (0.965)
  Pallas kernels: 91.4 us -> 88.2 us
    pallas_call x1, Pallas kernels: 89.7 us -> 86.6 us  [local(): pl.pallas_call(backward_kernel, out_shape=[pltpu.VMEM(a.shape, a.dtype) f...]
where the time goes in v6:
time: 89.1 us; the launch traced here: 89 us
  Pallas kernels  88.2 us (99%)
    pallas_call x1, Pallas kernels, local(): pl.pallas_call(backward_kernel, out_shape=[pltpu.VMEM(a.shape, a.dtype) f...  86.6 us

profile of v6, /device:TPU:16, one launch (start us, length us, event | category | flops | bytes accessed | tf_op | source)
XLA Modules:
  0.0 89.0 jit_solution(1848906291263301947)
XLA Ops:
  0.6 86.6 %backward.1 = (bf16[224,2048]{1,0:T(8,128)(2,1)S(1)}, bf16[224,2048]{1,0:T(8,128)(2,1)S(1)}, bf16[224,2048]{1,0:T(8,128)(2,1)S(1)}, f32[32,256]{1,0:T(8,128)S(1)...) custom-call(f32[1,256]{1,0:T(1,128)} %bitcast.20, s32[2,128]{1,0:T(2,128)} %bitcast.21, f32[2,128]{1,0:T(2,128)} %bitcast.22, ...), custom_call_target="tpu_custom_call" | custom-call | tf_op jit(solution)/shard_map/backward/pallas_call | solution.py:780
  87.2 1.6 %write_out.1 = (bf16[224,2048]{1,0:T(8,128)(2,1)}, bf16[224,2048]{1,0:T(8,128)(2,1)}, bf16[224,2048]{1,0:T(8,128)(2,1)}, f32[32,256]{1,0:T(8,128)}, bf16[128,256]{1,0:T(8,128)(2,1)}, /*index=5*/bf16[128,256]{1,0:T(8,128)(2,1)}) custom-call(bf16[224,2048]{1,0:T(8,128)(2,1)S(1)} %get-tuple-element.18.refs_0_, bf16[224,2048]{1,0:T(8,128)(2,1)S(1)} %get-tuple-element.19.refs_1_, ...), custom_call_target="tpu_custom_call" | custom-call | tf_op jit(solution)/shard_map/write_out/pallas_call | solution.py:847

commit v7 on v6

--- a/solution.py
+++ b/solution.py
@@ -30,11 +30,12 @@
     gg_ref, gu_ref, gd_ref, gp_ref, gv_ref, gt_ref,
     xq, cq, xq2, cq2, perm, sendbuf, sendbuf2, xc, wg, wu, wd, act_t, dg_t, du_t,
     part, sib_in, in_a, in_b, in_c, in_d, in_e, total, ret,
-    routes_ref, weight_ref, conv_ref, value_ref, gate_ref, taps_ref, res_ref, proj, normed, slope, mixed, scale, st_out, st_in, ext, halo_out, halo_in,
-    gp, gp_sib, gp_x, gp_row, gp_z,
+    routes_ref, weight_ref, conv_ref, value_ref, gate_ref, taps_ref, res_ref, proj, normed, slope, mixed, mixed2, scale, st_out, st_in, ext, halo_out, halo_in,
+    gp, gp_sib, gp_x, gp_row, gp_z, gp_z2, fin_out, fin_in,
     load_sem, own_sem, a2a_send, a2a_recv, far_send, far_recv, ag_send, ag_recv,
     sb_send, sb_recv, rs_send, rs_recv, ret_send, ret_recv, res_send, res_recv,
     st_send, st_recv, halo_sem, gs_send, gs_recv, gx_send, gx_recv, gz_send, gz_recv,
+    mx_sem, fin_sem, gz2_send, gz2_recv,
 ):
     sp = lax.axis_index("sp")
     y = lax.axis_index("tp")
@@ -600,6 +601,8 @@
     weight_grad(gd_ref, act_t, 1, 1)
     rs_close(0)
     rs_close(1)
+    mix_copy = remote(mixed, mixed2, mx_sem.at[0], mx_sem.at[1], dev_2)
+    mix_copy.start()
     drain_sums()
 
     all_in(ret.at[pl.ds(0, 240)], ret_recv.at[0])
@@ -637,6 +640,14 @@
         gp_copy(q, j).start()
         return mm(feats, proj[pl.ds(pl.multiple_of(q * 512, 512), 512), :], NN)
 
+    def cross_terms():
+        mix_copy.wait_recv()
+        term = mm(res_ref[y], mixed2[...], TN)
+        for i in range(8):
+            for cc in range(2):
+                gp[cc, i % 4, y2 * 2 + i // 4] = term[i * 64 + cc * 32 : i * 64 + cc * 32 + 32].astype(BF)
+        gp_copy(y2, 3).start()
+
     def gx_copy(q, j, i):
         return remote(
             gp.at[c, others_x[i], pair_of(q)], gp_x.at[i, pair_of(q)],
@@ -662,18 +673,30 @@
             + (gp_x[1, pair].astype(F32) + gp_x[2, pair].astype(F32))
         ).astype(BF)
         for i in range(2):
-
-            @pl.when(q * 2 + i != z)
-            def _():
-                gz_copy(q * 2 + i, z).start()
+            if j < 3:
+
+                @pl.when(q * 2 + i != z)
+                def _():
+                    gz_copy(q * 2 + i, z).start()
+
+            else:
+
+                @pl.when(y * 2 + i != z)
+                def _():
+                    remote(
+                        gp_row.at[q * 2 + i], gp_z2.at[z], gz2_send.at[0], gz2_recv.at[0],
+                        at_z(y * 2 + i),
+                    ).start()
 
     d_mixed = proj_terms(y, 0)
+    cross_terms()
+    over_x(y, 0)
+    over_x(y2, 3)
     for i in range(2):
         res_copy(ym, i, i, dev_m).wait_recv()
         res_copy(ym, i, 6, dev_p).start()
         res_copy(yp, 3 - i, 3 + i, dev_p).wait_recv()
         res_copy(yp, 3 - i, 7, dev_m).start()
-    over_x(y, 0)
     all_in(res_ref.at[ym, pl.ds(64, 64)], res_recv.at[2])
     d_mixed += proj_terms(ym, 1)
     all_in(res_ref.at[yp, pl.ds(0, 64)], res_recv.at[5])
@@ -682,7 +705,7 @@
     over_x(yp, 2)
     all_in(res_ref.at[y2, pl.ds(0, 64)], res_recv.at[6])
     all_in(res_ref.at[y2, pl.ds(64, 64)], res_recv.at[7])
-    d_mixed += proj_terms(y2, 3)
+    d_mixed += mm(res_ref[y2], proj[pl.ds(pl.multiple_of(y2 * 512, 512), 512), :], NN)
     d_norm = d_mixed * slope[...]
     norm_val = normed[...]
     stats2 = sums_out(
@@ -692,8 +715,8 @@
     )
     for copy in stats2:
         copy.start()
-    over_x(y2, 3)
     over_z(y, 0)
+    over_z(y2, 3)
 
     first_sum, second_sum = sums_in(1)
     conv_grad = (
@@ -723,18 +746,48 @@
     glu_grads(0, 64, correlate(0, 64))
     glu_grads(64, 32, correlate(64, 32))
 
-    over_z(y2, 3)
+    mine = z // 2
+    fin_copy = remote(fin_out, fin_in, fin_sem.at[0], fin_sem.at[1], dev_2)
+
+    @pl.when(mine == y)
+    def _():
+        all_in(gp_z2.at[pl.ds(0, 7)], gz2_recv.at[0])
+        cross = gp_row[y2 * 2 + lax.rem(z, 2)].astype(F32)
+        for k in range(1, 8):
+            cross += gp_z2[lax.rem(z + k, 8)].astype(F32)
+        fin_out[...] = cross
+        fin_copy.start()
+
     halo.wait_recv()
     keep = jnp.where(sp < 63, 1.0, 0.0)
     ext[128:160, :] = halo_in[...].astype(F32) * keep
     glu_grads(96, 32, correlate(96, 32))
 
-    all_in(gp_z.at[pl.ds(0, 7)], gz_recv.at[0])
-    rows_sum = gp_row[z].astype(F32)
-    for k in range(1, 8):
-        zz = lax.rem(z + k, 8)
-        rows_sum += gp_z[zz].astype(F32)
-    gp_ref[...] = rows_sum
+    @pl.when(mine != y2)
+    def _():
+        all_in(gp_z.at[pl.ds(0, 7)], gz_recv.at[0])
+        rows_sum = gp_row[z].astype(F32)
+        for k in range(1, 8):
+            rows_sum += gp_z[lax.rem(z + k, 8)].astype(F32)
+        gp_ref[...] = rows_sum
+        all_sent(gp_z.at[pl.ds(0, 5)], gz_send.at[0])
+
+    @pl.when(mine == y2)
+    def _():
+        fin_copy.wait_recv()
+        gp_ref[...] = fin_in[...]
+        all_sent(gp_z.at[pl.ds(0, 6)], gz_send.at[0])
+
+    @pl.when(mine == y)
+    def _():
+        fin_copy.wait_send()
+        all_sent(gp_z.at[pl.ds(0, 1)], gz2_send.at[0])
+
+    @pl.when(mine != y)
+    def _():
+        all_sent(gp_z.at[pl.ds(0, 2)], gz2_send.at[0])
+
+    mix_copy.wait_send()
 
     all_sent(ret.at[pl.ds(0, 240)], ret_send.at[0])
     for phase in range(2):
@@ -743,7 +796,6 @@
     all_sent(res_ref.at[pl.ds(0, 3)], res_send.at[0])
     all_sent(gp.at[oc], gs_send.at[0])
     all_sent(gp_x, gx_send.at[0])
-    all_sent(gp_z.at[pl.ds(0, 7)], gz_send.at[0])
 
 
 def write_kernel(*refs):
@@ -817,6 +869,7 @@
             pltpu.VMEM((128, 256), F32),
             pltpu.VMEM((128, 256), F32),
             pltpu.VMEM((128, 256), BF),
+            pltpu.VMEM((128, 256), BF),
             pltpu.VMEM((128, 256), F32),
             pltpu.VMEM((2, 8, 128), F32),
             pltpu.VMEM((2, 3, 8, 128), F32),
@@ -828,12 +881,16 @@
             pltpu.VMEM((3, 8, 32, 256), BF),
             pltpu.VMEM((8, 32, 256), BF),
             pltpu.VMEM((8, 32, 256), BF),
+            pltpu.VMEM((8, 32, 256), BF),
+            pltpu.VMEM((32, 256), F32),
+            pltpu.VMEM((32, 256), F32),
             dma((14,)), dma((4,)),
             dma((2,)), dma((2, 2)), dma((2,)), dma((2,)), dma((12,)), dma((4, 10)),
             dma((2,)), dma((2, 8)), dma((2, 2)), dma((2, 11)),
             dma((1,)), dma((1,)), dma((1,)), dma((8,)),
             dma((2,)), dma((2,)), dma((2,)),
             dma((1,)), dma((4,)), dma((1,)), dma((4,)), dma((1,)), dma((1,)),
+            dma((2,)), dma((2,)), dma((1,)), dma((1,)),
         ],
         compiler_params=pltpu.CompilerParams(
             collective_id=0, has_side_effects=True, vmem_limit_bytes=60 * 1024 * 1024

time: 89.1 us -> 88.7 us (level)
  no operation moved by 1% of the time
where the time goes in v7:
time: 88.7 us; the launch traced here: 88.6 us
  Pallas kernels  87.8 us (99%)
    pallas_call x1, Pallas kernels, local(): pl.pallas_call(backward_kernel, out_shape=[pltpu.VMEM(a.shape, a.dtype) f...  86.2 us

profile of v7, /device:TPU:16, one launch (start us, length us, event | category | flops | bytes accessed | tf_op | source)
XLA Modules:
  0.0 88.6 jit_solution(10855775018139217320)
XLA Ops:
  0.6 86.2 %backward.1 = (bf16[224,2048]{1,0:T(8,128)(2,1)S(1)}, bf16[224,2048]{1,0:T(8,128)(2,1)S(1)}, bf16[224,2048]{1,0:T(8,128)(2,1)S(1)}, f32[32,256]{1,0:T(8,128)S(1)...) custom-call(f32[1,256]{1,0:T(1,128)} %bitcast.20, s32[2,128]{1,0:T(2,128)} %bitcast.21, f32[2,128]{1,0:T(2,128)} %bitcast.22, ...), custom_call_target="tpu_custom_call" | custom-call | tf_op jit(solution)/shard_map/backward/pallas_call | solution.py:832
  86.9 1.6 %write_out.1 = (bf16[224,2048]{1,0:T(8,128)(2,1)}, bf16[224,2048]{1,0:T(8,128)(2,1)}, bf16[224,2048]{1,0:T(8,128)(2,1)}, f32[32,256]{1,0:T(8,128)}, bf16[128,256]{1,0:T(8,128)(2,1)}, /*index=5*/bf16[128,256]{1,0:T(8,128)(2,1)}) custom-call(bf16[224,2048]{1,0:T(8,128)(2,1)S(1)} %get-tuple-element.18.refs_0_, bf16[224,2048]{1,0:T(8,128)(2,1)S(1)} %get-tuple-element.19.refs_1_, ...), custom_call_target="tpu_custom_call" | custom-call | tf_op jit(solution)/shard_map/write_out/pallas_call | solution.py:904
